TPU v7x, 256 devices: a whole 4x4x8 slice. The times are simulated.
256 devices in a mesh: dp: 4 (over x), kv: 32 (over z, y), tp: 2 (over core).
Axes of the slice: x: 4, y: 4, z: 8, core: 2. Of those that a mesh axis runs over, the one named last changes fastest.
Arguments:
- tokens: bfloat16 [128, 4, 2048], P('dp', None, 'kv'), may hold values from -6 to 6
- in_gain: float32 [2048], P('kv'), may hold values from 0.1 to 1.9
- w_gate: bfloat16 [2048, 2048], P('kv', 'tp'), may hold values from -0.125 to 0.125
- w_value: bfloat16 [2048, 2048], P('kv', 'tp'), may hold values from -0.125 to 0.125
- w_key: bfloat16 [2048, 512], P('kv', 'tp'), may hold values from -0.125 to 0.125
- w_query: bfloat16 [2048, 512], P('kv', 'tp'), may hold values from -0.125 to 0.125
- w_step: bfloat16 [2048, 32], P('kv', 'tp'), may hold values from -0.125 to 0.125
- conv_value: bfloat16 [4, 2048], P(None, 'tp'), may hold values from -3 to 3
- conv_key: bfloat16 [4, 512], P(None, 'tp'), may hold values from -3 to 3
- conv_query: bfloat16 [4, 512], P(None, 'tp'), may hold values from -3 to 3
- step_bias: float32 [32], P('tp'), may hold values from -3 to 0
- decay_log: float32 [32], P('tp'), may hold values from -1 to 1.5
- out_gain: float32 [2048], P('tp'), may hold values from 0.1 to 1.9
- w_out: bfloat16 [2048, 2048], P('tp', 'kv'), may hold values from -0.125 to 0.125
- past_value: bfloat16 [128, 7, 2048], P(('dp', 'kv'), None, 'tp'), may hold values from -6 to 6
- past_key: bfloat16 [128, 7, 512], P(('dp', 'kv'), None, 'tp'), may hold values from -6 to 6
- past_query: bfloat16 [128, 7, 512], P(('dp', 'kv'), None, 'tp'), may hold values from -6 to 6
- past_states: float32 [128, 5, 32, 64, 128], P(('dp', 'kv'), None, 'tp'), may hold values from -2 to 2
- accepted: int32 [128], P(('dp', 'kv')), may hold values from 0 to 4
Outputs:
- mixed: bfloat16 [128, 4, 2048], P('dp', None, 'kv')
- new_states: float32 [128, 5, 32, 64, 128], P(('dp', 'kv'), None, 'tp')
- new_value: bfloat16 [128, 7, 2048], P(('dp', 'kv'), None, 'tp')
- new_key: bfloat16 [128, 7, 512], P(('dp', 'kv'), None, 'tp')
- new_query: bfloat16 [128, 7, 512], P(('dp', 'kv'), None, 'tp')
All inputs are finite; a program needn't handle non-finite values.
Results may differ from a plain program's by a relative error of at most 0.014.
Values may be sent and summed in bfloat16 or wider, within the bound.
No kernel may reach another device: no remote copies, remote signals or barrier semaphores. Data moves between devices by JAX's collectives and lax.ppermute only.
A program may use at most 64 MiB of HBM per device.

v0:
```python
import jax
import jax.numpy as jnp
from jax import lax
from jax.sharding import PartitionSpec as P

D = 2048
STATE = 128
CONV = 4
WIDTH = 2048


EPS = 1e-05


def in_blocks(shard, dim, length):
    before, after = (shard.shape[:dim], shard.shape[dim + 1 :])
    return jnp.moveaxis(shard.reshape(*before, length, -1, *after), dim, 0)


def sent_and_summed(shard, axis, dim):
    blocks = in_blocks(shard, dim, lax.axis_size(axis))
    arrived = lax.all_to_all(blocks, axis, split_axis=0, concat_axis=0, tiled=True)
    return arrived.astype(jnp.float32).sum(axis=0)


def side_by_side(arrays, axis, dim, along):
    columns = [a.reshape(*a.shape[:along], -1) for a in arrays]
    both = jnp.concatenate(columns, axis=along)
    filled, at, outs = (sent_and_summed(both, axis, dim), 0, [])
    for a, column in zip(arrays, columns):
        section = filled[..., at : at + column.shape[along]]
        outs.append(section.reshape(*section.shape[:along], *a.shape[along:]))
        at += column.shape[along]
    return tuple(outs)


def gathered_total(shard, axis):
    return lax.all_gather(shard, axis).sum(0)


def copy_for_each(shard, axis):
    length = lax.axis_size(axis)
    return lax.all_to_all(
        jnp.broadcast_to(shard[None], (length, *shard.shape)), axis, 0, 0, tiled=True
    )


def joined_along(blocks, dim):
    blocks = jnp.moveaxis(blocks, 0, dim)
    shape = blocks.shape
    return blocks.reshape(*shape[:dim], shape[dim] * shape[dim + 1], *shape[dim + 2 :])


def gather_directly(shard, axis, dim):
    blocks = copy_for_each(shard, axis)
    return joined_along(blocks, dim)


def of_everyone(shard, axis):
    everything = copy_for_each(shard, axis)
    return jnp.sum(everything.astype(jnp.float32), axis=0)


def take_window(history, offsets, span):
    return jax.vmap(lambda rows_one, offset: lax.dynamic_slice_in_dim(rows_one, offset, span, 0))(
        history, offsets
    )


def depthwise(history, taps, proposals):
    total = history[:, 0:proposals].astype(jnp.float32) * taps[0].astype(jnp.float32)
    for offset in range(1, taps.shape[0]):
        total = total + history[:, offset : offset + proposals].astype(jnp.float32) * taps[
            offset
        ].astype(jnp.float32)
    return jax.nn.silu(total)


def run_chain(values, keys, queries, steps, rates, initial, groups):
    seq_count, proposals, heads = steps.shape
    per_group = heads // groups
    head_dim = values.shape[2] // heads
    state_dim = keys.shape[2] // groups
    carried = initial.reshape(seq_count, groups, per_group, head_dim, state_dim)
    factor = jnp.exp(steps * rates)
    outputs = []
    saved = [initial]
    for position in range(proposals):
        moved = (
            values[:, position].reshape(seq_count, groups, per_group, head_dim)
            * steps[:, position].reshape(seq_count, groups, per_group)[..., None]
        )
        key_row = keys[:, position].reshape(seq_count, groups, state_dim)
        carried = (
            carried * factor[:, position].reshape(seq_count, groups, per_group)[..., None, None]
            + moved[..., None] * key_row[:, :, None, None, :]
        )
        query_row = queries[:, position].reshape(seq_count, groups, state_dim)
        result = jnp.einsum("sgrpn,sgn->sgrp", carried, query_row, precision=lax.Precision.HIGHEST)
        outputs.append(result.reshape(seq_count, heads * head_dim))
        saved.append(carried.reshape(seq_count, heads, head_dim, state_dim))
    return (jnp.stack(outputs, 1), jnp.stack(saved, 1))


def per_device(
    tokens,
    in_gain,
    w_gate,
    w_value,
    w_key,
    w_query,
    w_step,
    conv_value,
    conv_key,
    conv_query,
    step_bias,
    decay_log,
    out_gain,
    w_out,
    past_value,
    past_key,
    past_query,
    past_states,
    accepted,
):
    group_seqs, proposals, feature_slice = tokens.shape
    own_seqs = past_states.shape[0]
    rows_all = group_seqs * proposals
    own_rows = own_seqs * proposals
    widened = tokens.astype(jnp.float32)
    partial_squares = jnp.sum(widened * widened, axis=-1).reshape(rows_all)
    normed = (widened * in_gain).astype(jnp.bfloat16).reshape(rows_all, feature_slice)
    weights = (w_gate, w_value, w_key, w_query, w_step)

    def products():
        return jnp.concatenate(
            [jnp.dot(normed, weight, preferred_element_type=jnp.float32) for weight in weights],
            axis=1,
        )

    summed, own_squares = side_by_side(
        (products().astype(jnp.bfloat16), partial_squares.astype(jnp.bfloat16)), "kv", 0, 1
    )
    rscale = lax.rsqrt(own_squares / D + EPS)[:, None]
    scaled = (summed * rscale).reshape(own_seqs, proposals, -1)
    bounds = []
    offset = 0
    for weight in weights:
        bounds.append((offset, offset + weight.shape[1]))
        offset = offset + weight.shape[1]
    gate = scaled[:, :, bounds[0][0] : bounds[0][1]].astype(jnp.bfloat16)
    value = scaled[:, :, bounds[1][0] : bounds[1][1]].astype(jnp.bfloat16)
    key = scaled[:, :, bounds[2][0] : bounds[2][1]].astype(jnp.bfloat16)
    query = scaled[:, :, bounds[3][0] : bounds[3][1]].astype(jnp.bfloat16)
    raw_step = scaled[:, :, bounds[4][0] : bounds[4][1]]
    span = CONV - 1
    new_value = jnp.concatenate([take_window(past_value, accepted, span), value], axis=1)
    new_key = jnp.concatenate([take_window(past_key, accepted, span), key], axis=1)
    new_query = jnp.concatenate([take_window(past_query, accepted, span), query], axis=1)
    conv_v = depthwise(new_value, conv_value, proposals)
    conv_k = depthwise(new_key, conv_key, proposals)
    conv_q = depthwise(new_query, conv_query, proposals)
    steps = jax.nn.softplus(raw_step + step_bias)
    rates = -jnp.exp(decay_log)
    initial = jnp.take_along_axis(past_states, accepted[:, None, None, None, None], axis=1)[:, 0]
    local_groups = w_key.shape[1] // STATE
    mixed_heads, new_states = run_chain(conv_v, conv_k, conv_q, steps, rates, initial, local_groups)
    gated = mixed_heads * jax.nn.silu(gate.astype(jnp.float32))
    gate_squares = gathered_total(jnp.sum(gated * gated, axis=-1), "tp")
    scale_out = lax.rsqrt(gate_squares / WIDTH + EPS)[..., None]
    outn = (gated * scale_out * out_gain).astype(jnp.bfloat16).reshape(own_rows, -1)
    partial_out = jnp.dot(
        gather_directly(outn, "kv", 0), w_out, preferred_element_type=jnp.float32
    ).astype(jnp.bfloat16)
    total = of_everyone(partial_out.astype(jnp.float32).astype(jnp.bfloat16), "tp").astype(
        jnp.float32
    )
    mixed = total.astype(jnp.bfloat16).reshape(group_seqs, proposals, feature_slice)
    return (mixed, new_states, new_value, new_key, new_query)


def solution(mesh):
    placed = (
        P("dp", None, "kv"),
        P("kv"),
        P("kv", "tp"),
        P("kv", "tp"),
        P("kv", "tp"),
        P("kv", "tp"),
        P("kv", "tp"),
        P(None, "tp"),
        P(None, "tp"),
        P(None, "tp"),
        P("tp"),
        P("tp"),
        P("tp"),
        P("tp", "kv"),
        P(("dp", "kv"), None, "tp"),
        P(("dp", "kv"), None, "tp"),
        P(("dp", "kv"), None, "tp"),
        P(("dp", "kv"), None, "tp", None, None),
        P(("dp", "kv")),
    )
    return jax.shard_map(
        per_device,
        mesh=mesh,
        in_specs=placed,
        out_specs=(
            P("dp", None, "kv"),
            P(("dp", "kv"), None, "tp", None, None),
            P(("dp", "kv"), None, "tp"),
            P(("dp", "kv"), None, "tp"),
            P(("dp", "kv"), None, "tp"),
        ),
        check_vma=False,
    )
```

profile of v0, /device:TPU:1, one launch (start us, length us, event | category | flops | bytes accessed | tf_op | source)
XLA Modules:
  0.0 77.8 jit_solution(11776306234224267913)
XLA Ops:
  0.6 0.9 %fusion.24 = (bf16[32,4]{1,0:T(8,128)(2,1)S(1)}, bf16[32,4,64]{2,1,0:T(4,128)(2,1)S(1)}) fusion(bf16[32,4,64]{2,1,0:T(4,128)(2,1)} %param.19, f32[64]{0:T(128)} %param.20), kind=kLoop, calls=%fused_computation.41 | loop fusion | flops 40832 | bytes 33280 | tf_op jit(solution)/shard_map/reduce_sum | solution.py:131
  1.7 0.8 %convolution_convert_fusion.4 = bf16[32,4,16]{0,2,1:T(8,128)(2,1)S(1)} fusion(bf16[32,4,64]{2,1,0:T(4,128)(2,1)S(1)} %get-tuple-element.75, bf16[64,16]{0,1:T(8,128)(2,1)} %param.25), kind=kOutput, calls=%fused_computation.5 | convolution fusion | flops 264192 | bytes 22528 | tf_op jit(solution)/shard_map/dot_general | solution.py:137
  2.7 0.9 %convolution_convert_fusion.3 = bf16[32,4,256]{2,0,1:T(8,128)(2,1)S(1)} fusion(bf16[64,256]{1,0:T(8,128)(2,1)} %param.23, bf16[32,4,64]{2,1,0:T(4,128)(2,1)S(1)} %get-tuple-element.75), kind=kOutput, calls=%fused_computation.4 | convolution fusion | flops 4227072 | bytes 114688 | tf_op jit(solution)/shard_map/dot_general | solution.py:137
  3.7 0.9 %convolution_convert_fusion.2 = bf16[32,4,256]{2,0,1:T(8,128)(2,1)S(1)} fusion(bf16[64,256]{1,0:T(8,128)(2,1)} %param.24, bf16[32,4,64]{2,1,0:T(4,128)(2,1)S(1)} %get-tuple-element.75), kind=kOutput, calls=%fused_computation.3 | convolution fusion | flops 4227072 | bytes 114688 | tf_op jit(solution)/shard_map/dot_general | solution.py:137
  4.6 0.2 convolution_convert_fusion
  4.8 1.1 %convolution_convert_fusion.1 = bf16[32,4,1024]{2,0,1:T(8,128)(2,1)S(1)} fusion(bf16[64,1024]{1,0:T(8,128)(2,1)} %param.21, bf16[32,4,64]{2,1,0:T(4,128)(2,1)S(1)} %get-tuple-element.75), kind=kOutput, calls=%fused_computation.2 | convolution fusion | flops 16908288 | bytes 409600 | tf_op jit(solution)/shard_map/dot_general | solution.py:137
  6.0 0.3 concatenate.22
  6.3 1.2 %copy.77 = bf16[32,4,2577]{2,1,0:T(4,128)(2,1)} copy(bf16[32,4,2577]{2,0,1:T(8,128)(2,1)S(1)} %concatenate.22) | data formatting | bytes 1319424 | tf_op jit(solution)/shard_map/concatenate | solution.py:28
  7.5 12.0 %all-to-all-start = ((bf16[32,4,2577]{2,1,0:T(4,128)(2,1)}), bf16[32,4,2577]{2,1,0:T(4,128)(2,1)S(1)}, u32[]{:S(2)}, u32[]{:S(2)}) async-start(bf16[32,4,2577]{2,1,0:T(4,128)(2,1)} %copy.77), calls=%async_computation | async-start | bytes 1376256 | tf_op jit(solution)/shard_map/all_to_all | solution.py:22
  20.2 0.6 dynamic-slice.16
  21.5 2.0 %constant_dynamic-update-slice_fusion.1 = (f32[1,5,16,64,128]{4,3,2,1,0:T(8,128)}, f32[1,1,16,64,128]{4,3,2,1,0:T(8,128)S(1)}) fusion(f32[1,5,16,64,128]{4,3,2,1,0:T(8,128)} %param.36, s32[]{:T(128)} %bitcast.2, pred[]{:T(512)} %bitcast.1), kind=kLoop, calls=%fused_computation.67 | loop fusion | flops 131071 | bytes 1572869
  23.6 15.4 %all-to-all-done = bf16[32,4,2577]{2,1,0:T(4,128)(2,1)S(1)} async-done(((bf16[32,4,2577]{2,1,0:T(4,128)(2,1)}), bf16[32,4,2577]{2,1,0:T(4,128)(2,1)S(1)}, u32[]{:S(2)}, u32[]{:S(2)}) %all-to-all-start) | async-done | bytes 659744 | tf_op jit(solution)/shard_map/all_to_all | solution.py:22
  39.0 0.3 convert_reduce_fusion
  39.3 0.2 fusion.49
  40.4 0.6 pad_maximum_fusion
  41.7 1.4 %fusion.4 = f32[2,1,8,64]{3,1,2,0:T(1,128)S(1)} fusion(f32[2,8,64,128]{3,2,1,0:T(8,128)S(1)} %bitcast.113, f32[2,128]{1,0:T(2,128)S(1)} %bitcast.128, f32[2,8,64]{2,1,0:T(8,128)S(1)} %broadcast_multiply_fusion.7, f32[2,8]{1,0:T(2,128)S(1)} %mul.577, f32[1,4,256]{2,1,0:T(4,128)S(1)} %get-tuple-element.116), kind=kOutput, calls=%fused_computation.19 | convolution fusion | flops 1966080 | bytes 539648 | tf_op jit(solution)/shard_map/sgrpn,sgn->sgrp/dot_general | solution.py:99
  43.2 1.5 %fusion.20 = f32[2,1,8,64]{3,1,2,0:T(1,128)S(1)} fusion(f32[2,8,64,128]{3,2,1,0:T(8,128)S(1)} %bitcast.114, f32[2,128]{1,0:T(2,128)S(1)} %bitcast.142, f32[2,8,64]{2,1,0:T(8,128)S(1)} %broadcast_multiply_fusion.6, f32[2,8]{1,0:T(2,128)S(1)} %mul.614, f32[2,128]{1,0:T(2,128)S(1)} %bitcast.129, f32[2,8,64]{2,1,0:T(8,128)S(1)} %broadcast_multiply_fusion.7, ...), kind=kOutput, calls=%fused_computation.35 | convolution fusion | flops 2359296 | bytes 549888 | tf_op jit(solution)/shard_map/sgrpn,sgn->sgrp/dot_general | solution.py:99
  44.9 1.7 %fusion.5 = f32[2,1,8,64]{3,1,2,0:T(1,128)S(1)} fusion(f32[2,128]{1,0:T(2,128)S(1)} %bitcast.139, f32[2,8,64]{2,1,0:T(8,128)S(1)} %broadcast_multiply_fusion.5, f32[2,8]{1,0:T(2,128)S(1)} %mul.624, f32[2,8,64,128]{3,2,1,0:T(8,128)S(1)} %bitcast.115, f32[2,128]{1,0:T(2,128)S(1)} %bitcast.143, f32[2,8,64]{2,1,0:T(8,128)S(1)} %broadcast_multiply_fusion.6, ...), kind=kOutput, calls=%fused_computation.20 | convolution fusion | flops 2752512 | bytes 560128 | tf_op jit(solution)/shard_map/sgrpn,sgn->sgrp/dot_general | solution.py:99
  46.7 2.0 %fusion = f32[2,1,8,64]{3,1,2,0:T(1,128)S(1)} fusion(f32[2,128]{1,0:T(2,128)S(1)} %bitcast.137, f32[2,8,64]{2,1,0:T(8,128)S(1)} %broadcast_multiply_fusion.4, f32[2,8]{1,0:T(2,128)S(1)} %mul.634, f32[2,128]{1,0:T(2,128)S(1)} %bitcast.140, f32[2,8,64]{2,1,0:T(8,128)S(1)} %broadcast_multiply_fusion.5, f32[2,8]{1,0:T(2,128)S(1)} %mul.624, ...), kind=kOutput, calls=%fused_computation.12 | convolution fusion | flops 3145728 | bytes 570368 | tf_op jit(solution)/shard_map/sgrpn,sgn->sgrp/dot_general | solution.py:99
  48.9 0.2 dynamic-update-slice.4
  49.3 4.5 %all-reduce = f32[8]{0:T(128)S(1)} all-reduce(f32[8]{0:T(128)S(1)} %dynamic-update-slice.4), channel_id=2, replica_groups=mesh['dp'=4,'kv'=32,'tp'=2] {'tp'}, use_global_device_ids=true, to_apply=%add | all-reduce | flops 8 | bytes 64
  54.0 0.8 broadcast_in_dim.23
  54.8 4.7 %all-to-all-start.1 = ((bf16[32,4,1024]{2,1,0:T(4,128)(2,1)}), bf16[32,4,1024]{2,1,0:T(4,128)(2,1)S(1)}, u32[]{:S(2)}, u32[]{:S(2)}) async-start(bf16[32,4,1024]{2,1,0:T(4,128)(2,1)} %broadcast_in_dim.23), calls=%async_computation.1 | async-start | bytes 524288 | tf_op jit(solution)/shard_map/all_to_all | solution.py:43
  59.7 1.0 %fusion.6 = f32[1,5,16,64,128]{4,3,2,1,0:T(8,128)} fusion(f32[1,5,16,64,128]{4,3,2,1,0:T(8,128)} %get-tuple-element.66, f32[1,1,16,64,128]{4,3,2,1,0:T(8,128)S(1)} %get-tuple-element.67, f32[16,128]{1,0:T(8,128)S(1)} %broadcast_bitcast_fusion.3, f32[16,64]{1,0:T(8,128)S(1)} %broadcast_multiply_fusion.3, f32[16]{0:T(128)S(1)} %get-tuple-element.124), kind=kLoop, calls=%fused_computation.21 | loop fusion | flops 393216 | bytes 1060928
  60.8 1.2 %constant_dynamic-update-slice_fusion = f32[1,5,16,64,128]{4,3,2,1,0:T(8,128)} fusion(f32[1,5,16,64,128]{4,3,2,1,0:T(8,128)} %fusion.6, f32[16,128]{1,0:T(8,128)S(1)} %broadcast_bitcast_fusion.2, f32[16,64]{1,0:T(8,128)S(1)} %broadcast_multiply_fusion.2, f32[16]{0:T(128)S(1)} %get-tuple-element.123, f32[16,128]{1,0:T(8,128)S(1)} %broadcast_bitcast_fusion.3, ...), kind=kLoop, calls=%fused_computation.66 | loop fusion | flops 786432 | bytes 1073280
  62.0 0.6 pad_maximum_fusion.1
  62.6 1.4 %fusion.7 = f32[1,5,16,64,128]{4,3,2,1,0:T(8,128)} fusion(f32[1,5,16,64,128]{4,3,2,1,0:T(8,128)} %constant_dynamic-update-slice_fusion, f32[16,128]{1,0:T(8,128)S(1)} %broadcast_bitcast_fusion.1, f32[16,64]{1,0:T(8,128)S(1)} %broadcast_multiply_fusion.1, f32[16]{0:T(128)S(1)} %get-tuple-element.122, f32[16,128]{1,0:T(8,128)S(1)} %broadcast_bitcast_fusion.2, ...), kind=kLoop, calls=%fused_computation.22 | loop fusion | flops 1179648 | bytes 1085632
  63.9 1.5 %add_dynamic-update-slice_fusion = f32[1,5,16,64,128]{4,3,2,1,0:T(8,128)} fusion(f32[1,5,16,64,128]{4,3,2,1,0:T(8,128)} %fusion.7, f32[16,128]{1,0:T(8,128)S(1)} %broadcast_bitcast_fusion, f32[16,64]{1,0:T(8,128)S(1)} %broadcast_multiply_fusion, f32[16]{0:T(128)S(1)} %get-tuple-element.125, f32[16,128]{1,0:T(8,128)S(1)} %broadcast_bitcast_fusion.1, ...), kind=kLoop, calls=%fused_computation.8 | loop fusion | flops 1572864 | bytes 1097984 | tf_op jit(solution)/shard_map/stack | solution.py:102
  65.4 5.6 %all-to-all-done.1 = bf16[32,4,1024]{2,1,0:T(4,128)(2,1)S(1)} async-done(((bf16[32,4,1024]{2,1,0:T(4,128)(2,1)}), bf16[32,4,1024]{2,1,0:T(4,128)(2,1)S(1)}, u32[]{:S(2)}, u32[]{:S(2)}) %all-to-all-start.1) | async-done | bytes 262176 | tf_op jit(solution)/shard_map/all_to_all | solution.py:43
  71.1 0.2 convolution_convert_fusion.5
  71.4 5.7 %all_to_all.15 = bf16[2,128,64]{1,2,0:T(8,128)(2,1)S(1)} all-to-all(bf16[2,128,64]{1,2,0:T(8,128)(2,1)S(1)} %broadcast_in_dim.24), channel_id=1, replica_groups=mesh['dp'=4,'kv'=32,'tp'=2] {'tp'}, dimensions={0} | all-to-all | bytes 65536 | tf_op jit(solution)/shard_map/all_to_all | solution.py:43
  77.1 0.7 copy.78
  (84 shorter events, 3.3 us)
Async XLA Ops:
  0.6 4.0 %copy-start = (bf16[64,1024]{1,0:T(8,128)(2,1)S(1)}, bf16[64,1024]{1,0:T(8,128)(2,1)}, u32[]{:S(2)}) copy-start(bf16[64,1024]{1,0:T(8,128)(2,1)} %param.22) | copy-start | bytes 393220
  2.7 17.4 %copy-start.7 = (bf16[1,7,256]{2,1,0:T(8,128)(2,1)S(1)}, bf16[1,7,256]{2,1,0:T(8,128)(2,1)}, u32[]{:S(2)}) copy-start(bf16[1,7,256]{2,1,0:T(8,128)(2,1)} %param.34) | copy-start | bytes 10756
  3.6 16.6 %copy-start.11 = (u32[256]{0:T(256)S(1)}, u32[256]{0:T(256)}, u32[]{:S(2)}) copy-start(u32[256]{0:T(256)} %constant.132) | copy-start | bytes 3076
  3.7 17.8 %copy-start.8 = (bf16[1,7,256]{2,1,0:T(8,128)(2,1)S(1)}, bf16[1,7,256]{2,1,0:T(8,128)(2,1)}, u32[]{:S(2)}) copy-start(bf16[1,7,256]{2,1,0:T(8,128)(2,1)} %param.35) | copy-start | bytes 10756
  3.7 17.8 %copy-start.6 = (bf16[1,7,1024]{2,1,0:T(8,128)(2,1)S(1)}, bf16[1,7,1024]{2,1,0:T(8,128)(2,1)}, u32[]{:S(2)}) copy-start(bf16[1,7,1024]{2,1,0:T(8,128)(2,1)} %param.33) | copy-start | bytes 43012
  5.9 17.5 %copy-start.10 = (f32[16]{0:T(128)S(1)}, f32[16]{0:T(128)}, u32[]{:S(2)}) copy-start(f32[16]{0:T(128)} %param.30) | copy-start | bytes 196
  5.9 17.5 %copy-start.3 = (bf16[4,256]{1,0:T(4,128)(2,1)S(1)}, bf16[4,256]{1,0:T(4,128)(2,1)}, u32[]{:S(2)}) copy-start(bf16[4,256]{1,0:T(4,128)(2,1)} %param.27) | copy-start | bytes 6148
  6.0 17.6 %copy-start.4 = (bf16[4,256]{1,0:T(4,128)(2,1)S(1)}, bf16[4,256]{1,0:T(4,128)(2,1)}, u32[]{:S(2)}) copy-start(bf16[4,256]{1,0:T(4,128)(2,1)} %param.28) | copy-start | bytes 6148
  6.0 17.6 %copy-start.2 = (bf16[4,1024]{1,0:T(4,128)(2,1)S(1)}, bf16[4,1024]{1,0:T(4,128)(2,1)}, u32[]{:S(2)}) copy-start(bf16[4,1024]{1,0:T(4,128)(2,1)} %param.26) | copy-start | bytes 24580
  6.3 33.4 %copy-start.9 = (f32[16]{0:T(128)S(1)}, f32[16]{0:T(128)}, u32[]{:S(2)}) copy-start(f32[16]{0:T(128)} %param.29) | copy-start | bytes 196
  7.5 31.5 %all-to-all-start = ((bf16[32,4,2577]{2,1,0:T(4,128)(2,1)}), bf16[32,4,2577]{2,1,0:T(4,128)(2,1)S(1)}, u32[]{:S(2)}, u32[]{:S(2)}) async-start(bf16[32,4,2577]{2,1,0:T(4,128)(2,1)} %copy.77), calls=%async_computation | async-start | bytes 1376256 | tf_op jit(solution)/shard_map/all_to_all | solution.py:22
  41.5 12.4 %copy-start.5 = (f32[1024]{0:T(1024)S(1)}, f32[1024]{0:T(1024)}, u32[]{:S(2)}) copy-start(f32[1024]{0:T(1024)} %param.31) | copy-start | bytes 12292
  54.8 16.3 %all-to-all-start.1 = ((bf16[32,4,1024]{2,1,0:T(4,128)(2,1)}), bf16[32,4,1024]{2,1,0:T(4,128)(2,1)S(1)}, u32[]{:S(2)}, u32[]{:S(2)}) async-start(bf16[32,4,1024]{2,1,0:T(4,128)(2,1)} %broadcast_in_dim.23), calls=%async_computation.1 | async-start | bytes 524288 | tf_op jit(solution)/shard_map/all_to_all | solution.py:43
  59.4 11.7 %copy-start.1 = (bf16[1024,64]{0,1:T(8,128)(2,1)S(1)}, bf16[1024,64]{0,1:T(8,128)(2,1)}, u32[]{:S(2)}) copy-start(bf16[1024,64]{0,1:T(8,128)(2,1)} %param.32) | copy-start | bytes 393220
where the time goes:
time: 78.4 us; the launch traced here: 77.8 us
  waiting for transfers between devices  21.1 us (27%)
  starting transfers between devices  16.7 us (21%)
  other arithmetic  10.7 us (14%)
  matrix products  10.7 us (14%)
  blocking collectives  10.2 us (13%)
  local copies, waits for them, and re-layouts  6.03 us (8%)
  between operations  2.34 us (3%)
    all_to_all x1, waiting for transfers between devices, sent_and_summed(): lax.all_to_all(blocks, axis, split_axis=0, concat_axis=0, tiled=True)  15.4 us
    all_to_all x1, starting transfers between devices, sent_and_summed(): lax.all_to_all(blocks, axis, split_axis=0, concat_axis=0, tiled=True)  12 us
    dot_general x4, matrix products, run_chain(): jnp.einsum('sgrpn,sgn->sgrp', carried, query_row, precision=lax.Precision...  6.58 us
    all_to_all x1, blocking collectives, copy_for_each(): lax.all_to_all(jnp.broadcast_to(shard[None], (length, *shard.shape)), axi...  5.68 us
    all_to_all x1, waiting for transfers between devices, copy_for_each(): lax.all_to_all(jnp.broadcast_to(shard[None], (length, *shard.shape)), axi...  5.65 us
    unnamed x4, other arithmetic  5.54 us
    all_to_all x1, starting transfers between devices, copy_for_each(): lax.all_to_all(jnp.broadcast_to(shard[None], (length, *shard.shape)), axi...  4.67 us
    unnamed x1, blocking collectives  4.55 us
  transfers between devices with their start and end apart: 2, of which 2 were waited for; matrix products, arithmetic and copies ran while one was open for 11% of the time, Pallas kernels for 0%

commit v1 on v0

v1 whole, which is shorter than its diff:
```python
import jax
import jax.numpy as jnp
from jax import lax
from jax.experimental import pallas as pl
from jax.experimental.pallas import tpu as pltpu
from jax.sharding import PartitionSpec as P

D = 2048
CONV = 4
WIDTH = 2048
EPS = 1e-05

F32 = jnp.float32
BF16 = jnp.bfloat16
LANES = 128
VMEM = pltpu.VMEM
NT = (((1,), (1,)), ((), ()))


def local(x):
    return pltpu.with_memory_space_constraint(x, VMEM)


def lane_of(shape):
    return lax.broadcasted_iota(jnp.int32, shape, 1)


def halves(x):
    high = x.astype(BF16).astype(F32)
    return high, x - high


def project_kernel(tok, gain, wg, wv, wk, wq, ws, out, x_s, ws_s):
    seqs, prop, _ = tok.shape
    for i in range(seqs):
        x_s[prop * i : prop * (i + 1), :] = tok[i].astype(F32)
    ws_s[...] = jnp.zeros(ws_s.shape, BF16)
    ws_s[: ws.shape[0], :] = ws[...]
    x = x_s[...]
    squares = jnp.sum(x * x, axis=1, keepdims=True)
    normed = (x * gain[...]).astype(BF16)

    def put(at, product):
        width = product.shape[1]
        for i in range(seqs):
            out[i, :, at : at + width] = product[prop * i : prop * (i + 1)].astype(BF16)

    at = 0
    for w in (wg, wv, wk, wq):
        for c in range(0, w.shape[1], 256):
            put(at, jnp.dot(normed, w[:, c : c + 256], preferred_element_type=F32))
            at += 256
    heads = ws.shape[0]
    extra = lax.dot_general(normed, ws_s[...], NT, preferred_element_type=F32)
    high, low = halves(squares)
    lane = lane_of(extra.shape)
    extra = jnp.where(lane == heads, high, jnp.where(lane == heads + 1, low, extra))
    put(at, extra)


def project(tokens, gain, weights):
    seqs, prop, feat = tokens.shape
    columns = sum(w.shape[1] for w in weights[:4]) + LANES
    return pl.pallas_call(
        project_kernel,
        out_specs=pl.BlockSpec(memory_space=VMEM),
        out_shape=VMEM((seqs, prop, columns), BF16),
        scratch_shapes=[VMEM((seqs * prop, feat), F32), VMEM((LANES, feat), BF16)],
        name="project",
    )(tokens, gain.reshape(1, feat), *weights[:4], weights[4].T)


def prepare_kernel(
    accepted,
    states,
    past_v,
    past_k,
    past_q,
    taps_v,
    taps_k,
    taps_q,
    bias,
    log_rate,
    out_gain,
    state,
    state_high,
    state_low,
    rows,
    base,
    taps,
    bias_out,
    rate,
    gain,
    sem,
):
    offset = accepted[0]
    fetch = pltpu.make_async_copy(states.at[0, pl.ds(offset, 1)], state, sem)
    fetch.start()
    span, prop = rows.shape[0], base.shape[0]
    at = 0
    for past, tap in ((past_v, taps_v), (past_k, taps_k), (past_q, taps_q)):
        width = past.shape[2]
        history = past[0].astype(F32)
        picked = history[0:span]
        for j in range(1, history.shape[0] - span + 1):
            picked = jnp.where(offset == j, history[j : j + span], picked)
        weight = tap[...].astype(F32)
        rows[:, at : at + width] = picked
        taps[:, at : at + width] = weight
        for t in range(prop):
            part = jnp.zeros((1, width), F32)
            for i in range(CONV):
                if t + i < span:
                    part = part + picked[t + i : t + i + 1] * weight[i : i + 1]
            base[t : t + 1, at : at + width] = part
        at += width
    bias_out[...] = bias[...]
    rate[...] = -jnp.exp(log_rate[...])
    gain[...] = out_gain[...]
    fetch.wait()
    for h in range(state.shape[1]):
        at = slice(h * state.shape[2], (h + 1) * state.shape[2])
        high = state[0, h].astype(BF16)
        state_high[at] = high
        state_low[at] = (state[0, h] - high.astype(F32)).astype(BF16)


def prepare(accepted, states, pasts, taps, bias, log_rate, out_gain):
    _, _, heads, head_dim, state_dim = states.shape
    inner = heads * head_dim
    width = sum(p.shape[2] for p in pasts)
    prop = pasts[0].shape[1] - (CONV - 1)
    plain, vmem = pl.BlockSpec(), pl.BlockSpec(memory_space=VMEM)
    return pl.pallas_call(
        prepare_kernel,
        in_specs=[pl.BlockSpec(memory_space=pltpu.SMEM), pl.BlockSpec(memory_space=pl.ANY), *[plain] * 9],
        out_specs=[vmem] * 9,
        out_shape=[
            VMEM((1, heads, head_dim, state_dim), F32),
            VMEM((inner, state_dim), BF16),
            VMEM((inner, state_dim), BF16),
            VMEM((CONV - 1, width), F32),
            VMEM((prop, width), F32),
            VMEM((CONV, width), F32),
            VMEM((1, heads), F32),
            VMEM((1, heads), F32),
            VMEM((1, inner), F32),
        ],
        scratch_shapes=[pltpu.SemaphoreType.DMA(())],
        name="prepare",
    )(
        accepted,
        states,
        *pasts,
        *taps,
        bias.reshape(1, heads),
        log_rate.reshape(1, heads),
        out_gain.reshape(1, inner),
    )


def chain_kernel(
    arrived, state_high, state_low, base, taps, bias, rate, gain, sent, moved_out, key_out, decay_out, new_out
):
    copies, prop, _ = arrived.shape
    inner, state_dim = state_high.shape
    heads = bias.shape[1]
    head_dim = inner // heads
    width = base.shape[1]
    kwidth = (width - inner) // 2
    groups = kwidth // state_dim
    per_group = inner // groups

    total = arrived[0].astype(F32)
    for i in range(1, copies):
        total = total + arrived[i].astype(F32)
    at_step = inner + width
    squares = total[:, at_step + heads : at_step + heads + 1] + total[:, at_step + heads + 1 : at_step + heads + 2]
    rscale = lax.rsqrt(squares / D + EPS)

    def scaled(start, stop):
        return (total[:, start:stop] * rscale).astype(BF16).astype(F32)

    new = scaled(inner, at_step)
    new_out[...] = new
    filtered = base[...] + new * taps[CONV - 1 : CONV]
    for i in range(1, CONV):
        later = jnp.concatenate([jnp.zeros((i, width), F32), new[: prop - i]], axis=0)
        filtered = filtered + later * taps[CONV - 1 - i : CONV - i]
    convolved = filtered / (1.0 + jnp.exp(-filtered))
    conv_v, conv_k, conv_q = convolved[:, :inner], convolved[:, inner : inner + kwidth], convolved[:, inner + kwidth :]

    raw = total[:, at_step : at_step + heads] * rscale + bias[...]
    steps = jnp.maximum(raw, 0.0) + jnp.log1p(jnp.exp(-jnp.abs(raw)))
    decay = jnp.exp(steps * rate[...])
    first_half = lane_of((prop, 2 * head_dim)) < head_dim

    def spread(x):
        return jnp.concatenate(
            [jnp.where(first_half, x[:, h : h + 1], x[:, h + 1 : h + 2]) for h in range(0, heads, 2)], axis=1
        )

    moved = spread(steps) * conv_v
    shrink = spread(decay)
    moved_out[0:prop, :] = moved
    moved_out[prop:, :] = jnp.zeros((moved_out.shape[0] - prop, inner), F32)
    key_out[...] = conv_k
    decay_out[...] = decay

    q_high, q_low = halves(conv_q)
    q_both = jnp.concatenate([q_high, q_low], axis=0).astype(BF16)
    row = lax.broadcasted_iota(jnp.int32, (prop, per_group), 0)
    ys = []
    for g in range(groups):
        cols = slice(g * per_group, (g + 1) * per_group)
        part = slice(g * state_dim, (g + 1) * state_dim)
        main = lax.dot_general(q_both[:, part], state_high[cols], NT, preferred_element_type=F32)
        rest = lax.dot_general(q_both[:prop, part], state_low[cols], NT, preferred_element_type=F32)
        carried = main[:prop] + main[prop:] + rest
        y = jnp.zeros((prop, per_group), F32)
        for t in range(prop):
            match = jnp.sum(conv_q[:, part] * conv_k[t : t + 1, part], axis=1, keepdims=True)
            carried = carried * shrink[t : t + 1, cols] + moved[t : t + 1, cols] * match
            y = jnp.where(row == t, carried, y)
        ys.append(y)
    y = jnp.concatenate(ys, axis=1)
    gate = scaled(0, inner)
    u = (y * (gate / (1.0 + jnp.exp(-gate))) * gain[...]).astype(BF16)
    for i in range(copies):
        sent[i] = u


def chain(arrived, state_high, state_low, base, taps, bias, rate, gain):
    copies, prop, _ = arrived.shape
    inner, heads, width = state_high.shape[0], bias.shape[1], base.shape[1]
    vmem = pl.BlockSpec(memory_space=VMEM)
    return pl.pallas_call(
        chain_kernel,
        in_specs=[vmem] * 8,
        out_specs=[vmem] * 5,
        out_shape=[
            VMEM((copies, prop, inner), BF16),
            VMEM((8, inner), F32),
            VMEM((prop, (width - inner) // 2), F32),
            VMEM((prop, heads), F32),
            VMEM((prop, width), F32),
        ],
        name="chain",
    )(*map(local, (arrived, state_high, state_low, base, taps, bias, rate, gain)))


def states_kernel(
    first, moved, keys, decay, rows, new, new_states, new_v, new_k, new_q, state_s, moved_s, sem_out
):
    prop, heads = decay.shape
    _, _, head_dim, state_dim = state_s.shape
    inner, kwidth = moved.shape[1], keys.shape[1]
    per_group = heads * state_dim // kwidth
    writes = []

    def write(source, slot):
        copy = pltpu.make_async_copy(source, new_states.at[0, slot], sem_out.at[slot])
        copy.start()
        writes.append(copy)

    write(first.at[0], 0)
    at = 0
    for out in (new_v, new_k, new_q):
        width = out.shape[2]
        both = jnp.concatenate([rows[:, at : at + width], new[:, at : at + width]], axis=0)
        out[0] = both.astype(BF16)
        at += width
    for c in range(0, inner, LANES):
        moved_s[c : c + LANES, :] = jnp.transpose(moved[:, c : c + LANES])
    for t in range(prop):
        for h in range(heads):
            g = h // per_group
            before = first[0, h] if t == 0 else state_s[t - 1, h]
            key_row = keys[t : t + 1, g * state_dim : (g + 1) * state_dim]
            column = moved_s[h * head_dim : (h + 1) * head_dim, t : t + 1]
            state_s[t, h] = before * decay[t : t + 1, h : h + 1] + column * key_row
        write(state_s.at[t], t + 1)
    for copy in writes:
        copy.wait()


def next_states(keep, first, moved, keys, decay, rows, new):
    _, heads, head_dim, state_dim = first.shape
    inner, kwidth = moved.shape[1], keys.shape[1]
    count = rows.shape[0] + new.shape[0]
    plain = pl.BlockSpec()
    vmem = pl.BlockSpec(memory_space=VMEM)
    return pl.pallas_call(
        states_kernel,
        in_specs=[vmem] * 6,
        out_specs=[pl.BlockSpec(memory_space=pl.ANY), plain, plain, plain],
        out_shape=[
            jax.ShapeDtypeStruct((1, keep, heads, head_dim, state_dim), F32),
            jax.ShapeDtypeStruct((1, count, inner), BF16),
            jax.ShapeDtypeStruct((1, count, kwidth), BF16),
            jax.ShapeDtypeStruct((1, count, kwidth), BF16),
        ],
        scratch_shapes=[
            VMEM((keep - 1, heads, head_dim, state_dim), F32),
            VMEM((inner, 8), F32),
            pltpu.SemaphoreType.DMA((keep,)),
        ],
        name="states",
    )(*map(local, (first, moved, keys, decay, rows, new)))


def output_kernel(rows, w_out, gain, out):
    features = w_out.shape[0]
    x = rows[...]
    out[:, :features] = lax.dot_general(x, w_out[...], NT, preferred_element_type=F32).astype(BF16)
    wide = x.astype(F32)
    inverse = 1.0 / (gain[...] * gain[...])
    squares = jnp.sum(wide * wide * inverse, axis=1, keepdims=True)
    high, low = halves(squares)
    lane = lane_of((x.shape[0], LANES - features))
    out[:, features:] = jnp.where(lane == 0, high, jnp.where(lane == 1, low, 0.0)).astype(BF16)


def output(rows, w_out, gain):
    vmem = pl.BlockSpec(memory_space=VMEM)
    return pl.pallas_call(
        output_kernel,
        in_specs=[vmem] * 3,
        out_specs=vmem,
        out_shape=VMEM((rows.shape[0], LANES), BF16),
        name="output",
    )(local(rows), local(w_out.T), local(gain))


def combine_kernel(mine, other, out):
    seqs, prop, features = out.shape
    a, b = mine[...].astype(F32), other[...].astype(F32)
    squares_a = a[:, features : features + 1] + a[:, features + 1 : features + 2]
    squares_b = b[:, features : features + 1] + b[:, features + 1 : features + 2]
    scale = lax.rsqrt((squares_a + squares_b) / WIDTH + EPS)
    mixed = (a[:, :features] + b[:, :features]) * scale
    for i in range(seqs):
        out[i] = mixed[prop * i : prop * (i + 1)].astype(BF16)


def combine(mine, other, seqs, features):
    vmem = pl.BlockSpec(memory_space=VMEM)
    return pl.pallas_call(
        combine_kernel,
        in_specs=[vmem, vmem],
        out_shape=jax.ShapeDtypeStruct((seqs, mine.shape[0] // seqs, features), BF16),
        name="combine",
    )(local(mine), local(other))


def per_device(
    tokens,
    in_gain,
    w_gate,
    w_value,
    w_key,
    w_query,
    w_step,
    conv_value,
    conv_key,
    conv_query,
    step_bias,
    decay_log,
    out_gain,
    w_out,
    past_value,
    past_key,
    past_query,
    past_states,
    accepted,
):
    group_seqs, proposals, features = tokens.shape
    partial = project(tokens, in_gain, (w_gate, w_value, w_key, w_query, w_step))
    arrived = lax.all_to_all(partial, "kv", 0, 0, tiled=True)
    first, high, low, rows, base, taps, bias, rate, gain = prepare(
        accepted,
        past_states,
        (past_value, past_key, past_query),
        (conv_value, conv_key, conv_query),
        step_bias,
        decay_log,
        out_gain,
    )
    sent, moved, keys, decay, new = chain(arrived, high, low, base, taps, bias, rate, gain)
    gathered = lax.all_to_all(sent, "kv", 0, 0, tiled=True)
    saved = next_states(past_states.shape[1], first, moved, keys, decay, rows, new)
    mine = output(gathered.reshape(group_seqs * proposals, -1), w_out, gain)
    swap = [(i, 1 - i) for i in range(2)]
    mixed = combine(mine, lax.ppermute(mine, "tp", swap), group_seqs, features)
    return (mixed, *saved)


def solution(mesh):
    placed = (
        P("dp", None, "kv"),
        P("kv"),
        P("kv", "tp"),
        P("kv", "tp"),
        P("kv", "tp"),
        P("kv", "tp"),
        P("kv", "tp"),
        P(None, "tp"),
        P(None, "tp"),
        P(None, "tp"),
        P("tp"),
        P("tp"),
        P("tp"),
        P("tp", "kv"),
        P(("dp", "kv"), None, "tp"),
        P(("dp", "kv"), None, "tp"),
        P(("dp", "kv"), None, "tp"),
        P(("dp", "kv"), None, "tp", None, None),
        P(("dp", "kv")),
    )
    return jax.shard_map(
        per_device,
        mesh=mesh,
        in_specs=placed,
        out_specs=(
            P("dp", None, "kv"),
            P(("dp", "kv"), None, "tp", None, None),
            P(("dp", "kv"), None, "tp"),
            P(("dp", "kv"), None, "tp"),
            P(("dp", "kv"), None, "tp"),
        ),
        check_vma=False,
    )
```

time: 78.4 us -> 58.2 us (0.74)
  matrix products: 10.7 us -> 0 us
  other arithmetic: 10.7 us -> 0 us
  Pallas kernels: 0 us -> 8.14 us
  local copies, waits for them, and re-layouts: 6.03 us -> 0.07 us
  blocking collectives: 10.2 us -> 15.6 us
  waiting for transfers between devices: 21.1 us -> 16.8 us
  between operations: 2.34 us -> 1.38 us
  starting transfers between devices: 16.7 us -> 15.9 us
    dot_general x10 -> x0, matrix products: 10.7 us -> none  [the longest x4 6.58 us: run_chain(): jnp.einsum('sgrpn,sgn->sgrp', carried, query_row, precision=lax.Precision...]
    all_to_all x1, blocking collectives: 5.68 us -> 15.6 us  [per_device(): gathered = lax.all_to_all(sent, 'kv', 0, 0, tiled=True)]
    pallas_call x0 -> x6, Pallas kernels: none -> 8.14 us  [the longest x1 2.47 us: next_states(): pl.pallas_call(states_kernel, in_specs=[vmem] * 6, out_specs=[pl.BlockSpe...]
    unnamed x4 -> x0, other arithmetic: 5.54 us -> none
    all_to_all x2 -> x1, starting transfers between devices: 16.7 us -> 12 us  [per_device(): arrived = lax.all_to_all(partial, 'kv', 0, 0, tiled=True)]
    unnamed x1 -> x0, blocking collectives: 4.55 us -> none
    all_to_all x2 -> x1, waiting for transfers between devices: 21.1 us -> 16.8 us  [per_device(): arrived = lax.all_to_all(partial, 'kv', 0, 0, tiled=True)]
    ppermute x0 -> x1, starting transfers between devices: none -> 3.85 us  [per_device(): mixed = combine(mine, lax.ppermute(mine, 'tp', swap), group_seqs, features)]
  transfers between devices with their start and end apart: 2 -> 2, of which waited for: 2 -> 1; matrix products, arithmetic and copies ran while one was open for 11% -> 0% of each run, Pallas kernels for 0% -> 8%
where the time goes in v1:
time: 58.2 us; the launch traced here: 57.9 us
  waiting for transfers between devices  16.8 us (29%)
  starting transfers between devices  15.9 us (27%)
  blocking collectives  15.6 us (27%)
  Pallas kernels  8.14 us (14%)
  between operations  1.38 us (2%)
    all_to_all x1, waiting for transfers between devices, per_device(): arrived = lax.all_to_all(partial, 'kv', 0, 0, tiled=True)  16.8 us
    all_to_all x1, blocking collectives, per_device(): gathered = lax.all_to_all(sent, 'kv', 0, 0, tiled=True)  15.6 us
    all_to_all x1, starting transfers between devices, per_device(): arrived = lax.all_to_all(partial, 'kv', 0, 0, tiled=True)  12 us
    ppermute x1, starting transfers between devices, per_device(): mixed = combine(mine, lax.ppermute(mine, 'tp', swap), group_seqs, features)  3.85 us
    pallas_call x1, Pallas kernels, next_states(): pl.pallas_call(states_kernel, in_specs=[vmem] * 6, out_specs=[pl.BlockSpe...  2.47 us
    pallas_call x1, Pallas kernels, project(): pl.pallas_call(project_kernel, out_specs=pl.BlockSpec(memory_space=VMEM),...  2.21 us
    pallas_call x1, Pallas kernels, prepare(): pl.pallas_call(prepare_kernel, in_specs=[pl.BlockSpec(memory_space=pltpu....  1.96 us
  transfers between devices with their start and end apart: 2, of which 1 were waited for; matrix products, arithmetic and copies ran while one was open for 0% of the time, Pallas kernels for 8%

profile of v1, /device:TPU:1, one launch (start us, length us, event | category | flops | bytes accessed | tf_op | source)
XLA Modules:
  0.0 57.9 jit_solution(7871670898978427262)
XLA Ops:
  0.6 2.2 %project.1 = bf16[32,4,2688]{2,1,0:T(4,128)(2,1)} custom-call(bf16[32,4,64]{2,1,0:T(4,128)(2,1)} %tok.1, f32[1,64]{1,0:T(1,128)} %bitcast.9, bf16[64,1024]{1,0:T(8,128)(2,1)} %wg.1, bf16[64,1024]{1,0:T(8,128)(2,1)} %wv.1, bf16[64,256]{1,0:T(8,128)(2,1)} %wk.1, bf16[64,256]{1,0:T(8,128)(2,1)} %wq.1, bf16[16,64]{1,0:T(8,128)(2,1)} %bitcast.7), custom_call_target="tpu_custom_call" | custom-call | tf_op jit(solution)/shard_map/project/pallas_call | solution.py:64
  2.8 12.0 %all-to-all-start = ((bf16[32,4,2688]{2,1,0:T(4,128)(2,1)}), bf16[32,4,2688]{2,1,0:T(4,128)(2,1)S(1)}, u32[]{:S(2)}, u32[]{:S(2)}) async-start(bf16[32,4,2688]{2,1,0:T(4,128)(2,1)} %project.1), calls=%async_computation | async-start | bytes 1376256 | tf_op jit(solution)/shard_map/all_to_all | solution.py:379
  14.9 0.0 copy-start
  15.6 2.0 %prepare.1 = (f32[1,16,64,128]{3,2,1,0:T(8,128)S(1)}, bf16[1024,128]{1,0:T(8,128)(2,1)S(1)}, bf16[1024,128]{1,0:T(8,128)(2,1)S(1)}, f32[3,1536]{1,0:T(4,128)S(1)...) custom-call(s32[1]{0:T(128)S(6)} %copy.24.accepted, ...), custom_call_target="tpu_custom_call" | custom-call | tf_op jit(solution)/shard_map/prepare/pallas_call | solution.py:134
  17.5 16.8 %all-to-all-done.arrived = bf16[32,4,2688]{2,1,0:T(4,128)(2,1)S(1)} async-done(((bf16[32,4,2688]{2,1,0:T(4,128)(2,1)}), bf16[32,4,2688]{2,1,0:T(4,128)(2,1)S(1)}, u32[]{:S(2)}, u32[]{:S(2)}) %all-to-all-start) | async-done | bytes 688160 | tf_op jit(solution)/shard_map/all_to_all | solution.py:379
  34.3 0.5 chain.1
  34.8 15.6 %all_to_all.10 = bf16[32,4,1024]{2,1,0:T(4,128)(2,1)S(1)} all-to-all(bf16[32,4,1024]{2,1,0:T(4,128)(2,1)S(1)} %get-tuple-element.30), channel_id=1, replica_groups=mesh['dp'=4,'kv'=32,'tp'=2] {'kv'}, dimensions={0} | all-to-all | bytes 524288 | tf_op jit(solution)/shard_map/all_to_all | solution.py:390
  50.4 0.1 reshape.29.rows
  50.5 0.0 copy-done
  50.5 0.3 output.1.mine
  50.8 3.8 %collective-permute-start = (bf16[128,128]{1,0:T(8,128)(2,1)S(1)}, bf16[128,128]{1,0:T(8,128)(2,1)S(1)}, u32[]{:S(2)}, u32[]{:S(2)}) collective-permute-start(bf16[128,128]{1,0:T(8,128)(2,1)S(1)} %output.1.mine), channel_id=1, source_target_pairs={{0,1},{1,0},{2,3},{3,2},{4,5},{5,4},{6,7},{7,6},{8,9},{9,8},{10,11... | collective-permute-start | bytes 98312 | tf_op jit(solution)/shard_map/ppermute | solution.py:394
  54.6 2.5 %states.3 = (f32[1,5,16,64,128]{4,3,2,1,0:T(8,128)}, bf16[1,7,1024]{2,1,0:T(8,128)(2,1)}, bf16[1,7,256]{2,1,0:T(8,128)(2,1)}, bf16[1,7,256]{2,1,0:T(8,128)(2,1)}) custom-call(f32[1,16,64,128]{3,2,1,0:T(8,128)S(1)} %get-tuple-element.31.first, f32[8,1024]{1,0:T(8,128)S(1)} %get-tuple-element.32.moved, f32[4,256]{1,0:T(4,128)S(1)} %get-tuple-element.33.keys, ...), custom_call_target="tpu_custom_call" | custom-call | tf_op jit(solution)/shard_map/states/pallas_call | solution.py:293
  57.1 0.0 collective-permute-done.other
  57.1 0.8 %combine.1 = bf16[32,4,64]{2,1,0:T(4,128)(2,1)} custom-call(bf16[128,128]{1,0:T(8,128)(2,1)S(1)} %output.1.mine, bf16[128,128]{1,0:T(8,128)(2,1)S(1)} %collective-permute-done.other), custom_call_target="tpu_custom_call" | custom-call | tf_op jit(solution)/shard_map/combine/pallas_call | solution.py:348
Async XLA Ops:
  2.8 31.5 %all-to-all-start = ((bf16[32,4,2688]{2,1,0:T(4,128)(2,1)}), bf16[32,4,2688]{2,1,0:T(4,128)(2,1)S(1)}, u32[]{:S(2)}, u32[]{:S(2)}) async-start(bf16[32,4,2688]{2,1,0:T(4,128)(2,1)} %project.1), calls=%async_computation | async-start | bytes 1376256 | tf_op jit(solution)/shard_map/all_to_all | solution.py:379
  14.9 35.6 %copy-start = (bf16[1024,64]{0,1:T(8,128)(2,1)S(1)}, bf16[1024,64]{0,1:T(8,128)(2,1)}, u32[]{:S(2)}) copy-start(bf16[1024,64]{0,1:T(8,128)(2,1)} %param.32) | copy-start | bytes 393220
  50.8 6.3 %collective-permute-start = (bf16[128,128]{1,0:T(8,128)(2,1)S(1)}, bf16[128,128]{1,0:T(8,128)(2,1)S(1)}, u32[]{:S(2)}, u32[]{:S(2)}) collective-permute-start(bf16[128,128]{1,0:T(8,128)(2,1)S(1)} %output.1.mine), channel_id=1, source_target_pairs={{0,1},{1,0},{2,3},{3,2},{4,5},{5,4},{6,7},{7,6},{8,9},{9,8},{10,11... | collective-permute-start | bytes 98312 | tf_op jit(solution)/shard_map/ppermute | solution.py:394

commit v2 on v1

--- a/solution.py
+++ b/solution.py
@@ -1,3 +1,5 @@
+import functools
+
 import jax
 import jax.numpy as jnp
 from jax import lax
@@ -9,6 +11,8 @@
 CONV = 4
 WIDTH = 2048
 EPS = 1e-05
+KV = ("kz", "ky")
+NEAR = 4
 
 F32 = jnp.float32
 BF16 = jnp.bfloat16
@@ -32,8 +36,11 @@
 
 def project_kernel(tok, gain, wg, wv, wk, wq, ws, out, x_s, ws_s):
     seqs, prop, _ = tok.shape
+    near, block, _ = out.shape
+    far = seqs // near
     for i in range(seqs):
-        x_s[prop * i : prop * (i + 1), :] = tok[i].astype(F32)
+        at = prop * ((i % near) * far + i // near)
+        x_s[at : at + prop, :] = tok[i].astype(F32)
     ws_s[...] = jnp.zeros(ws_s.shape, BF16)
     ws_s[: ws.shape[0], :] = ws[...]
     x = x_s[...]
@@ -42,8 +49,9 @@
 
     def put(at, product):
         width = product.shape[1]
-        for i in range(seqs):
-            out[i, :, at : at + width] = product[prop * i : prop * (i + 1)].astype(BF16)
+        rounded = product.astype(BF16)
+        for j in range(near):
+            out[j, :, at : at + width] = rounded[block * j : block * (j + 1)]
 
     at = 0
     for w in (wg, wv, wk, wq):
@@ -52,22 +60,51 @@
             at += 256
     heads = ws.shape[0]
     extra = lax.dot_general(normed, ws_s[...], NT, preferred_element_type=F32)
+    put(at, with_squares(extra, squares, heads))
+
+
+def with_squares(extra, squares, at):
     high, low = halves(squares)
     lane = lane_of(extra.shape)
-    extra = jnp.where(lane == heads, high, jnp.where(lane == heads + 1, low, extra))
-    put(at, extra)
-
-
-def project(tokens, gain, weights):
+    return jnp.where(lane == at, high, jnp.where(lane == at + 1, low, extra))
+
+
+def project(tokens, gain, weights, near):
     seqs, prop, feat = tokens.shape
     columns = sum(w.shape[1] for w in weights[:4]) + LANES
     return pl.pallas_call(
         project_kernel,
         out_specs=pl.BlockSpec(memory_space=VMEM),
-        out_shape=VMEM((seqs, prop, columns), BF16),
+        out_shape=VMEM((near, seqs // near * prop, columns), BF16),
         scratch_shapes=[VMEM((seqs * prop, feat), F32), VMEM((LANES, feat), BF16)],
         name="project",
     )(tokens, gain.reshape(1, feat), *weights[:4], weights[4].T)
+
+
+def fold_kernel(heads, arrived, out):
+    near, _, columns = arrived.shape
+    far, prop, _ = out.shape
+    for at in range(0, columns, LANES):
+        total = arrived[0, :, at : at + LANES].astype(F32)
+        for j in range(1, near):
+            total = total + arrived[j, :, at : at + LANES].astype(F32)
+        if at == columns - LANES:
+            squares = total[:, heads : heads + 1] + total[:, heads + 1 : heads + 2]
+            total = with_squares(total, squares, heads)
+        for k in range(far):
+            out[k, :, at : at + LANES] = total[prop * k : prop * (k + 1)].astype(BF16)
+
+
+def fold(arrived, far, heads):
+    _, rows, columns = arrived.shape
+    vmem = pl.BlockSpec(memory_space=VMEM)
+    return pl.pallas_call(
+        functools.partial(fold_kernel, heads),
+        in_specs=[vmem],
+        out_specs=vmem,
+        out_shape=VMEM((far, rows // far, columns), BF16),
+        name="fold",
+    )(local(arrived))
 
 
 def prepare_kernel(
@@ -226,12 +263,12 @@
     y = jnp.concatenate(ys, axis=1)
     gate = scaled(0, inner)
     u = (y * (gate / (1.0 + jnp.exp(-gate))) * gain[...]).astype(BF16)
-    for i in range(copies):
+    for i in range(sent.shape[0]):
         sent[i] = u
 
 
-def chain(arrived, state_high, state_low, base, taps, bias, rate, gain):
-    copies, prop, _ = arrived.shape
+def chain(copies, arrived, state_high, state_low, base, taps, bias, rate, gain):
+    prop = arrived.shape[1]
     inner, heads, width = state_high.shape[0], bias.shape[1], base.shape[1]
     vmem = pl.BlockSpec(memory_space=VMEM)
     return pl.pallas_call(
@@ -375,8 +412,9 @@
     accepted,
 ):
     group_seqs, proposals, features = tokens.shape
-    partial = project(tokens, in_gain, (w_gate, w_value, w_key, w_query, w_step))
-    arrived = lax.all_to_all(partial, "kv", 0, 0, tiled=True)
+    weights = (w_gate, w_value, w_key, w_query, w_step)
+    partial = project(tokens, in_gain, weights, lax.axis_size("ky"))
+    nearby = lax.all_to_all(partial, "ky", 0, 0, tiled=True)
     first, high, low, rows, base, taps, bias, rate, gain = prepare(
         accepted,
         past_states,
@@ -386,8 +424,10 @@
         decay_log,
         out_gain,
     )
-    sent, moved, keys, decay, new = chain(arrived, high, low, base, taps, bias, rate, gain)
-    gathered = lax.all_to_all(sent, "kv", 0, 0, tiled=True)
+    partial = fold(nearby, lax.axis_size("kz"), w_step.shape[1])
+    arrived = lax.all_to_all(partial, "kz", 0, 0, tiled=True)
+    sent, moved, keys, decay, new = chain(group_seqs, arrived, high, low, base, taps, bias, rate, gain)
+    gathered = lax.all_to_all(sent, KV, 0, 0, tiled=True)
     saved = next_states(past_states.shape[1], first, moved, keys, decay, rows, new)
     mine = output(gathered.reshape(group_seqs * proposals, -1), w_out, gain)
     swap = [(i, 1 - i) for i in range(2)]
@@ -396,37 +436,40 @@
 
 
 def solution(mesh):
+    dp, kv, tp = mesh.devices.shape
+    near = NEAR if kv % NEAR == 0 else 1
+    split = jax.sharding.Mesh(mesh.devices.reshape(dp, kv // near, near, tp), ("dp", *KV, "tp"))
     placed = (
-        P("dp", None, "kv"),
-        P("kv"),
-        P("kv", "tp"),
-        P("kv", "tp"),
-        P("kv", "tp"),
-        P("kv", "tp"),
-        P("kv", "tp"),
+        P("dp", None, KV),
+        P(KV),
+        P(KV, "tp"),
+        P(KV, "tp"),
+        P(KV, "tp"),
+        P(KV, "tp"),
+        P(KV, "tp"),
         P(None, "tp"),
         P(None, "tp"),
         P(None, "tp"),
         P("tp"),
         P("tp"),
         P("tp"),
-        P("tp", "kv"),
-        P(("dp", "kv"), None, "tp"),
-        P(("dp", "kv"), None, "tp"),
-        P(("dp", "kv"), None, "tp"),
-        P(("dp", "kv"), None, "tp", None, None),
-        P(("dp", "kv")),
+        P("tp", KV),
+        P(("dp", *KV), None, "tp"),
+        P(("dp", *KV), None, "tp"),
+        P(("dp", *KV), None, "tp"),
+        P(("dp", *KV), None, "tp", None, None),
+        P(("dp", *KV)),
     )
     return jax.shard_map(
         per_device,
-        mesh=mesh,
+        mesh=split,
         in_specs=placed,
         out_specs=(
-            P("dp", None, "kv"),
-            P(("dp", "kv"), None, "tp", None, None),
-            P(("dp", "kv"), None, "tp"),
-            P(("dp", "kv"), None, "tp"),
-            P(("dp", "kv"), None, "tp"),
+            P("dp", None, KV),
+            P(("dp", *KV), None, "tp", None, None),
+            P(("dp", *KV), None, "tp"),
+            P(("dp", *KV), None, "tp"),
+            P(("dp", *KV), None, "tp"),
         ),
         check_vma=False,
     )

time: 58.2 us -> 57.2 us (0.983)
  blocking collectives: 15.6 us -> 28.4 us
  waiting for transfers between devices: 16.8 us -> 5.86 us
  starting transfers between devices: 15.9 us -> 13 us
    all_to_all x1 -> x2, blocking collectives: 15.6 us -> 28.4 us  [the longest x1 14.9 us: per_device(): nearby = lax.all_to_all(partial, 'ky', 0, 0, tiled=True)]
    all_to_all x1, waiting for transfers between devices: 16.8 us -> 5.85 us  [per_device(): arrived = lax.all_to_all(partial, 'kz', 0, 0, tiled=True)]
    all_to_all x1, starting transfers between devices: 12 us -> 8.31 us  [per_device(): arrived = lax.all_to_all(partial, 'kz', 0, 0, tiled=True)]
    pallas_call x0 -> x1, Pallas kernels: none -> 0.85 us  [fold(): pl.pallas_call(functools.partial(fold_kernel, heads), in_specs=[vmem], ou...]
    pallas_call x1, Pallas kernels: 2.21 us -> 1.36 us  [project(): pl.pallas_call(project_kernel, out_specs=pl.BlockSpec(memory_space=VMEM),...]
    ppermute x1, starting transfers between devices: 3.85 us -> 4.66 us  [per_device(): mixed = combine(mine, lax.ppermute(mine, 'tp', swap), group_seqs, features)]
where the time goes in v2:
time: 57.2 us; the launch traced here: 56.8 us
  blocking collectives  28.4 us (50%)
  starting transfers between devices  13 us (23%)
  Pallas kernels  8.12 us (14%)
  waiting for transfers between devices  5.86 us (10%)
  between operations  1.35 us (2%)
    all_to_all x1, blocking collectives, per_device(): nearby = lax.all_to_all(partial, 'ky', 0, 0, tiled=True)  14.9 us
    all_to_all x1, blocking collectives, per_device(): gathered = lax.all_to_all(sent, KV, 0, 0, tiled=True)  13.6 us
    all_to_all x1, starting transfers between devices, per_device(): arrived = lax.all_to_all(partial, 'kz', 0, 0, tiled=True)  8.31 us
    all_to_all x1, waiting for transfers between devices, per_device(): arrived = lax.all_to_all(partial, 'kz', 0, 0, tiled=True)  5.85 us
    ppermute x1, starting transfers between devices, per_device(): mixed = combine(mine, lax.ppermute(mine, 'tp', swap), group_seqs, features)  4.66 us
    pallas_call x1, Pallas kernels, next_states(): pl.pallas_call(states_kernel, in_specs=[vmem] * 6, out_specs=[pl.BlockSpe...  2.47 us
    pallas_call x1, Pallas kernels, prepare(): pl.pallas_call(prepare_kernel, in_specs=[pl.BlockSpec(memory_space=pltpu....  1.96 us
    pallas_call x1, Pallas kernels, project(): pl.pallas_call(project_kernel, out_specs=pl.BlockSpec(memory_space=VMEM),...  1.36 us
  transfers between devices with their start and end apart: 2, of which 1 were waited for; matrix products, arithmetic and copies ran while one was open for 0% of the time, Pallas kernels for 8%

profile of v2, /device:TPU:1, one launch (start us, length us, event | category | flops | bytes accessed | tf_op | source)
XLA Modules:
  0.0 56.8 jit_solution(2681048453302378253)
XLA Ops:
  0.6 1.4 %project.1 = bf16[4,32,2688]{2,1,0:T(8,128)(2,1)S(1)} custom-call(bf16[32,4,64]{2,1,0:T(4,128)(2,1)} %tok.1, f32[1,64]{1,0:T(1,128)} %bitcast.9, bf16[64,1024]{1,0:T(8,128)(2,1)} %wg.1, bf16[64,1024]{1,0:T(8,128)(2,1)} %wv.1, bf16[64,256]{1,0:T(8,128)(2,1)} %wk.1, bf16[64,256]{1,0:T(8,128)(2,1)} %wq.1, bf16[16,64]{1,0:T(8,128)(2,1)} %bitcast.7), custom_call_target="tpu_custom_call" | custom-call | tf_op jit(solution)/shard_map/project/pallas_call | solution.py:75
  2.0 14.9 %all_to_all.15.arrived = bf16[4,32,2688]{2,1,0:T(8,128)(2,1)S(1)} all-to-all(bf16[4,32,2688]{2,1,0:T(8,128)(2,1)S(1)} %project.1), channel_id=1, replica_groups=mesh['dp'=4,'kz'=8,'ky'=4,'tp'=2] {'ky'}, dimensions={0} | all-to-all | bytes 1376256 | tf_op jit(solution)/shard_map/all_to_all | solution.py:417
  16.9 0.9 %fold.1 = bf16[8,4,2688]{2,1,0:T(4,128)(2,1)} custom-call(bf16[4,32,2688]{2,1,0:T(8,128)(2,1)S(1)} %all_to_all.15.arrived), custom_call_target="tpu_custom_call" | custom-call | tf_op jit(solution)/shard_map/fold/pallas_call | solution.py:101
  17.7 0.0 copy-start
  17.7 8.3 %all-to-all-start.1 = ((bf16[8,4,2688]{2,1,0:T(4,128)(2,1)}), bf16[8,4,2688]{2,1,0:T(4,128)(2,1)S(1)}, u32[]{:S(2)}, u32[]{:S(2)}) async-start(bf16[8,4,2688]{2,1,0:T(4,128)(2,1)} %fold.1), calls=%async_computation.1 | async-start | bytes 344064 | tf_op jit(solution)/shard_map/all_to_all | solution.py:428
  26.7 2.0 %prepare.1 = (f32[1,16,64,128]{3,2,1,0:T(8,128)S(1)}, bf16[1024,128]{1,0:T(8,128)(2,1)S(1)}, bf16[1024,128]{1,0:T(8,128)(2,1)S(1)}, f32[3,1536]{1,0:T(4,128)S(1)...) custom-call(s32[1]{0:T(128)S(6)} %copy.24.accepted, ...), custom_call_target="tpu_custom_call" | custom-call | tf_op jit(solution)/shard_map/prepare/pallas_call | solution.py:171
  28.7 5.9 %all-to-all-done.1.arrived = bf16[8,4,2688]{2,1,0:T(4,128)(2,1)S(1)} async-done(((bf16[8,4,2688]{2,1,0:T(4,128)(2,1)}), bf16[8,4,2688]{2,1,0:T(4,128)(2,1)S(1)}, u32[]{:S(2)}, u32[]{:S(2)}) %all-to-all-start.1) | async-done | bytes 172064 | tf_op jit(solution)/shard_map/all_to_all | solution.py:428
  34.5 0.4 chain.1
  35.0 13.6 %all_to_all.16 = bf16[32,4,1024]{2,1,0:T(4,128)(2,1)S(1)} all-to-all(bf16[32,4,1024]{2,1,0:T(4,128)(2,1)S(1)} %get-tuple-element.30), channel_id=1, replica_groups=mesh['dp'=4,'kz'=8,'ky'=4,'tp'=2] {'kz','ky'}, dimensions={0} | all-to-all | bytes 524288 | tf_op jit(solution)/shard_map/all_to_all | solution.py:430
  48.5 0.1 reshape.29.rows
  48.6 0.0 copy-done
  48.6 0.3 output.1.mine
  48.9 4.7 %collective-permute-start = (bf16[128,128]{1,0:T(8,128)(2,1)S(1)}, bf16[128,128]{1,0:T(8,128)(2,1)S(1)}, u32[]{:S(2)}, u32[]{:S(2)}) collective-permute-start(bf16[128,128]{1,0:T(8,128)(2,1)S(1)} %output.1.mine), channel_id=1, source_target_pairs={{0,1},{1,0},{2,3},{3,2},{4,5},{5,4},{6,7},{7,6},{8,9},{9,8},{10,11... | collective-permute-start | bytes 98312 | tf_op jit(solution)/shard_map/ppermute | solution.py:434
  53.5 2.5 %states.3 = (f32[1,5,16,64,128]{4,3,2,1,0:T(8,128)}, bf16[1,7,1024]{2,1,0:T(8,128)(2,1)}, bf16[1,7,256]{2,1,0:T(8,128)(2,1)}, bf16[1,7,256]{2,1,0:T(8,128)(2,1)}) custom-call(f32[1,16,64,128]{3,2,1,0:T(8,128)S(1)} %get-tuple-element.31.first, f32[8,1024]{1,0:T(8,128)S(1)} %get-tuple-element.32.moved, f32[4,256]{1,0:T(4,128)S(1)} %get-tuple-element.33.keys, ...), custom_call_target="tpu_custom_call" | custom-call | tf_op jit(solution)/shard_map/states/pallas_call | solution.py:330
  56.0 0.0 collective-permute-done.other
  56.0 0.8 %combine.1 = bf16[32,4,64]{2,1,0:T(4,128)(2,1)} custom-call(bf16[128,128]{1,0:T(8,128)(2,1)S(1)} %output.1.mine, bf16[128,128]{1,0:T(8,128)(2,1)S(1)} %collective-permute-done.other), custom_call_target="tpu_custom_call" | custom-call | tf_op jit(solution)/shard_map/combine/pallas_call | solution.py:385
Async XLA Ops:
  17.7 30.9 %copy-start = (bf16[1024,64]{0,1:T(8,128)(2,1)S(1)}, bf16[1024,64]{0,1:T(8,128)(2,1)}, u32[]{:S(2)}) copy-start(bf16[1024,64]{0,1:T(8,128)(2,1)} %param.32) | copy-start | bytes 393220
  17.7 16.8 %all-to-all-start.1 = ((bf16[8,4,2688]{2,1,0:T(4,128)(2,1)}), bf16[8,4,2688]{2,1,0:T(4,128)(2,1)S(1)}, u32[]{:S(2)}, u32[]{:S(2)}) async-start(bf16[8,4,2688]{2,1,0:T(4,128)(2,1)} %fold.1), calls=%async_computation.1 | async-start | bytes 344064 | tf_op jit(solution)/shard_map/all_to_all | solution.py:428
  48.9 7.1 %collective-permute-start = (bf16[128,128]{1,0:T(8,128)(2,1)S(1)}, bf16[128,128]{1,0:T(8,128)(2,1)S(1)}, u32[]{:S(2)}, u32[]{:S(2)}) collective-permute-start(bf16[128,128]{1,0:T(8,128)(2,1)S(1)} %output.1.mine), channel_id=1, source_target_pairs={{0,1},{1,0},{2,3},{3,2},{4,5},{5,4},{6,7},{7,6},{8,9},{9,8},{10,11... | collective-permute-start | bytes 98312 | tf_op jit(solution)/shard_map/ppermute | solution.py:434

commit v3 on v2

--- a/solution.py
+++ b/solution.py
@@ -34,18 +34,42 @@
     return high, x - high
 
 
-def project_kernel(tok, gain, wg, wv, wk, wq, ws, out, x_s, ws_s):
+def with_squares(extra, squares, at):
+    high, low = halves(squares)
+    lane = lane_of(extra.shape)
+    return jnp.where(lane == at, high, jnp.where(lane == at + 1, low, extra))
+
+
+def first_kernel(*refs):
+    sources, results, scratch = refs[:18], refs[18:28], refs[28:]
+    accepted, states, *plain = sources
+    out, state, state_high, state_low, rows, base, taps, bias, rate, gain = results
+    accepted_s, tok, in_gain, wg, wv, wk, wq, ws, pv, pk, pq, tv, tk, tq, log_rate, x_s, ws_s, sems = scratch
+
+    def copy(source, target, slot):
+        moving = pltpu.make_async_copy(source, target, sems.at[slot])
+        moving.start()
+        return moving
+
+    offset_copy = copy(accepted, accepted_s, 0)
+    targets = (tok, in_gain, wg, wv, wk, wq, ws, pv, pk, pq, tv, tk, tq, bias, log_rate, gain)
+    copies = [copy(source, target, 2 + n) for n, (source, target) in enumerate(zip(plain, targets))]
+    ws_s[...] = jnp.zeros(ws_s.shape, BF16)
+    offset_copy.wait()
+    offset = accepted_s[0, 0]
+    fetch = copy(states.at[0, pl.ds(offset, 1)], state, 1)
+
+    copies[0].wait()
+    copies[1].wait()
     seqs, prop, _ = tok.shape
     near, block, _ = out.shape
     far = seqs // near
     for i in range(seqs):
         at = prop * ((i % near) * far + i // near)
         x_s[at : at + prop, :] = tok[i].astype(F32)
-    ws_s[...] = jnp.zeros(ws_s.shape, BF16)
-    ws_s[: ws.shape[0], :] = ws[...]
     x = x_s[...]
     squares = jnp.sum(x * x, axis=1, keepdims=True)
-    normed = (x * gain[...]).astype(BF16)
+    normed = (x * in_gain[...]).astype(BF16)
 
     def put(at, product):
         width = product.shape[1]
@@ -54,88 +78,23 @@
             out[j, :, at : at + width] = rounded[block * j : block * (j + 1)]
 
     at = 0
-    for w in (wg, wv, wk, wq):
+    for n, w in enumerate((wg, wv, wk, wq)):
+        copies[2 + n].wait()
         for c in range(0, w.shape[1], 256):
             put(at, jnp.dot(normed, w[:, c : c + 256], preferred_element_type=F32))
             at += 256
+    copies[6].wait()
     heads = ws.shape[0]
+    ws_s[:heads, :] = ws[...]
     extra = lax.dot_general(normed, ws_s[...], NT, preferred_element_type=F32)
     put(at, with_squares(extra, squares, heads))
 
-
-def with_squares(extra, squares, at):
-    high, low = halves(squares)
-    lane = lane_of(extra.shape)
-    return jnp.where(lane == at, high, jnp.where(lane == at + 1, low, extra))
-
-
-def project(tokens, gain, weights, near):
-    seqs, prop, feat = tokens.shape
-    columns = sum(w.shape[1] for w in weights[:4]) + LANES
-    return pl.pallas_call(
-        project_kernel,
-        out_specs=pl.BlockSpec(memory_space=VMEM),
-        out_shape=VMEM((near, seqs // near * prop, columns), BF16),
-        scratch_shapes=[VMEM((seqs * prop, feat), F32), VMEM((LANES, feat), BF16)],
-        name="project",
-    )(tokens, gain.reshape(1, feat), *weights[:4], weights[4].T)
-
-
-def fold_kernel(heads, arrived, out):
-    near, _, columns = arrived.shape
-    far, prop, _ = out.shape
-    for at in range(0, columns, LANES):
-        total = arrived[0, :, at : at + LANES].astype(F32)
-        for j in range(1, near):
-            total = total + arrived[j, :, at : at + LANES].astype(F32)
-        if at == columns - LANES:
-            squares = total[:, heads : heads + 1] + total[:, heads + 1 : heads + 2]
-            total = with_squares(total, squares, heads)
-        for k in range(far):
-            out[k, :, at : at + LANES] = total[prop * k : prop * (k + 1)].astype(BF16)
-
-
-def fold(arrived, far, heads):
-    _, rows, columns = arrived.shape
-    vmem = pl.BlockSpec(memory_space=VMEM)
-    return pl.pallas_call(
-        functools.partial(fold_kernel, heads),
-        in_specs=[vmem],
-        out_specs=vmem,
-        out_shape=VMEM((far, rows // far, columns), BF16),
-        name="fold",
-    )(local(arrived))
-
-
-def prepare_kernel(
-    accepted,
-    states,
-    past_v,
-    past_k,
-    past_q,
-    taps_v,
-    taps_k,
-    taps_q,
-    bias,
-    log_rate,
-    out_gain,
-    state,
-    state_high,
-    state_low,
-    rows,
-    base,
-    taps,
-    bias_out,
-    rate,
-    gain,
-    sem,
-):
-    offset = accepted[0]
-    fetch = pltpu.make_async_copy(states.at[0, pl.ds(offset, 1)], state, sem)
-    fetch.start()
-    span, prop = rows.shape[0], base.shape[0]
+    for n in range(7, 16):
+        copies[n].wait()
+    rate[...] = -jnp.exp(log_rate[...])
+    span = rows.shape[0]
     at = 0
-    for past, tap in ((past_v, taps_v), (past_k, taps_k), (past_q, taps_q)):
+    for past, tap in ((pv, tv), (pk, tk), (pq, tq)):
         width = past.shape[2]
         history = past[0].astype(F32)
         picked = history[0:span]
@@ -151,9 +110,7 @@
                     part = part + picked[t + i : t + i + 1] * weight[i : i + 1]
             base[t : t + 1, at : at + width] = part
         at += width
-    bias_out[...] = bias[...]
-    rate[...] = -jnp.exp(log_rate[...])
-    gain[...] = out_gain[...]
+
     fetch.wait()
     for h in range(state.shape[1]):
         at = slice(h * state.shape[2], (h + 1) * state.shape[2])
@@ -162,17 +119,21 @@
         state_low[at] = (state[0, h] - high.astype(F32)).astype(BF16)
 
 
-def prepare(accepted, states, pasts, taps, bias, log_rate, out_gain):
+def first(near, accepted, states, tokens, in_gain, weights, pasts, taps, bias, log_rate, out_gain):
+    seqs, prop, feat = tokens.shape
     _, _, heads, head_dim, state_dim = states.shape
     inner = heads * head_dim
     width = sum(p.shape[2] for p in pasts)
-    prop = pasts[0].shape[1] - (CONV - 1)
-    plain, vmem = pl.BlockSpec(), pl.BlockSpec(memory_space=VMEM)
-    return pl.pallas_call(
-        prepare_kernel,
-        in_specs=[pl.BlockSpec(memory_space=pltpu.SMEM), pl.BlockSpec(memory_space=pl.ANY), *[plain] * 9],
-        out_specs=[vmem] * 9,
+    columns = sum(w.shape[1] for w in weights[:4]) + LANES
+    row = (tokens, in_gain.reshape(1, feat), *weights[:4], weights[4].T, *pasts, *taps)
+    row = (*row, bias.reshape(1, heads), log_rate.reshape(1, heads), out_gain.reshape(1, inner))
+    landing = [VMEM(x.shape, x.dtype) for x in row]
+    return pl.pallas_call(
+        first_kernel,
+        in_specs=[pl.BlockSpec(memory_space=pltpu.HBM)] * 18,
+        out_specs=[pl.BlockSpec(memory_space=VMEM)] * 10,
         out_shape=[
+            VMEM((near, seqs // near * prop, columns), BF16),
             VMEM((1, heads, head_dim, state_dim), F32),
             VMEM((inner, state_dim), BF16),
             VMEM((inner, state_dim), BF16),
@@ -183,17 +144,42 @@
             VMEM((1, heads), F32),
             VMEM((1, inner), F32),
         ],
-        scratch_shapes=[pltpu.SemaphoreType.DMA(())],
-        name="prepare",
-    )(
-        accepted,
-        states,
-        *pasts,
-        *taps,
-        bias.reshape(1, heads),
-        log_rate.reshape(1, heads),
-        out_gain.reshape(1, inner),
-    )
+        scratch_shapes=[
+            pltpu.SMEM((1, 1), jnp.int32),
+            *landing[:13],
+            landing[14],
+            VMEM((seqs * prop, feat), F32),
+            VMEM((LANES, feat), BF16),
+            pltpu.SemaphoreType.DMA((18,)),
+        ],
+        name="first",
+    )(accepted.reshape(1, 1), states, *row)
+
+
+def fold_kernel(heads, arrived, out):
+    near, _, columns = arrived.shape
+    far, prop, _ = out.shape
+    for at in range(0, columns, LANES):
+        total = arrived[0, :, at : at + LANES].astype(F32)
+        for j in range(1, near):
+            total = total + arrived[j, :, at : at + LANES].astype(F32)
+        if at == columns - LANES:
+            squares = total[:, heads : heads + 1] + total[:, heads + 1 : heads + 2]
+            total = with_squares(total, squares, heads)
+        for k in range(far):
+            out[k, :, at : at + LANES] = total[prop * k : prop * (k + 1)].astype(BF16)
+
+
+def fold(arrived, far, heads):
+    _, rows, columns = arrived.shape
+    vmem = pl.BlockSpec(memory_space=VMEM)
+    return pl.pallas_call(
+        functools.partial(fold_kernel, heads),
+        in_specs=[vmem],
+        out_specs=vmem,
+        out_shape=VMEM((far, rows // far, columns), BF16),
+        name="fold",
+    )(local(arrived))
 
 
 def chain_kernel(
@@ -412,23 +398,25 @@
     accepted,
 ):
     group_seqs, proposals, features = tokens.shape
-    weights = (w_gate, w_value, w_key, w_query, w_step)
-    partial = project(tokens, in_gain, weights, lax.axis_size("ky"))
-    nearby = lax.all_to_all(partial, "ky", 0, 0, tiled=True)
-    first, high, low, rows, base, taps, bias, rate, gain = prepare(
+    partial, state, high, low, rows, base, taps, bias, rate, gain = first(
+        lax.axis_size("ky"),
         accepted,
         past_states,
+        tokens,
+        in_gain,
+        (w_gate, w_value, w_key, w_query, w_step),
         (past_value, past_key, past_query),
         (conv_value, conv_key, conv_query),
         step_bias,
         decay_log,
         out_gain,
     )
+    nearby = lax.all_to_all(partial, "ky", 0, 0, tiled=True)
     partial = fold(nearby, lax.axis_size("kz"), w_step.shape[1])
     arrived = lax.all_to_all(partial, "kz", 0, 0, tiled=True)
     sent, moved, keys, decay, new = chain(group_seqs, arrived, high, low, base, taps, bias, rate, gain)
     gathered = lax.all_to_all(sent, KV, 0, 0, tiled=True)
-    saved = next_states(past_states.shape[1], first, moved, keys, decay, rows, new)
+    saved = next_states(past_states.shape[1], state, moved, keys, decay, rows, new)
     mine = output(gathered.reshape(group_seqs * proposals, -1), w_out, gain)
     swap = [(i, 1 - i) for i in range(2)]
     mixed = combine(mine, lax.ppermute(mine, "tp", swap), group_seqs, features)

time: 57.2 us -> 57.6 us (level)
  blocking collectives: 28.4 us -> 45 us
  starting transfers between devices: 13 us -> 4.66 us
  waiting for transfers between devices: 5.86 us -> 0.01 us
  Pallas kernels: 8.12 us -> 6.26 us
    all_to_all x0 -> x1, blocking collectives: none -> 16.4 us  [per_device(): arrived = lax.all_to_all(partial, 'kz', 0, 0, tiled=True)]
    all_to_all x1 -> x0, starting transfers between devices: 8.31 us -> none  [per_device(): arrived = lax.all_to_all(partial, 'kz', 0, 0, tiled=True)]
    all_to_all x1 -> x0, waiting for transfers between devices: 5.85 us -> none  [per_device(): arrived = lax.all_to_all(partial, 'kz', 0, 0, tiled=True)]
    pallas_call x2 -> x1, Pallas kernels: 3.32 us -> 2.13 us  [first(): pl.pallas_call(first_kernel, in_specs=[pl.BlockSpec(memory_space=pltpu.HB...]
    pallas_call x1, Pallas kernels: 0.85 us -> 0.19 us  [fold(): pl.pallas_call(functools.partial(fold_kernel, heads), in_specs=[vmem], ou...]
  transfers between devices with their start and end apart: 2 -> 1, of which waited for: 1 -> 0; matrix products, arithmetic and copies ran while one was open for 0% -> 0% of each run, Pallas kernels for 8% -> 4%
where the time goes in v3:
time: 57.6 us; the launch traced here: 57.4 us
  blocking collectives  45 us (78%)
  Pallas kernels  6.26 us (11%)
  starting transfers between devices  4.66 us (8%)
  between operations  1.35 us (2%)
    all_to_all x1, blocking collectives, per_device(): arrived = lax.all_to_all(partial, 'kz', 0, 0, tiled=True)  16.4 us
    all_to_all x1, blocking collectives, per_device(): nearby = lax.all_to_all(partial, 'ky', 0, 0, tiled=True)  15 us
    all_to_all x1, blocking collectives, per_device(): gathered = lax.all_to_all(sent, KV, 0, 0, tiled=True)  13.6 us
    ppermute x1, starting transfers between devices, per_device(): mixed = combine(mine, lax.ppermute(mine, 'tp', swap), group_seqs, features)  4.66 us
    pallas_call x1, Pallas kernels, next_states(): pl.pallas_call(states_kernel, in_specs=[vmem] * 6, out_specs=[pl.BlockSpe...  2.47 us
    pallas_call x1, Pallas kernels, first(): pl.pallas_call(first_kernel, in_specs=[pl.BlockSpec(memory_space=pltpu.HB...  2.13 us
  transfers between devices with their start and end apart: 1, of which 0 were waited for; matrix products, arithmetic and copies ran while one was open for 0% of the time, Pallas kernels for 4%

profile of v3, /device:TPU:1, one launch (start us, length us, event | category | flops | bytes accessed | tf_op | source)
XLA Modules:
  0.0 57.4 jit_solution(4608921277274432108)
XLA Ops:
  1.3 2.1 %first.1 = (bf16[4,32,2688]{2,1,0:T(8,128)(2,1)S(1)}, f32[1,16,64,128]{3,2,1,0:T(8,128)S(1)}, bf16[1024,128]{1,0:T(8,128)(2,1)S(1)}, bf16[1024,128]{1,0:T(8,128)...) custom-call(s32[1,1]{1,0:T(1,128)} %bitcast.7.refs_0_, ...), custom_call_target="tpu_custom_call" | custom-call | tf_op jit(solution)/shard_map/first/pallas_call | solution.py:131
  3.4 0.0 copy-start
  3.4 15.0 %all_to_all.15.arrived = bf16[4,32,2688]{2,1,0:T(8,128)(2,1)S(1)} all-to-all(bf16[4,32,2688]{2,1,0:T(8,128)(2,1)S(1)} %get-tuple-element.24), channel_id=1, replica_groups=mesh['dp'=4,'kz'=8,'ky'=4,'tp'=2] {'ky'}, dimensions={0} | all-to-all | bytes 1376256 | tf_op jit(solution)/shard_map/all_to_all | solution.py:414
  18.5 0.2 fold.1
  18.7 16.4 %all_to_all.16.arrived = bf16[8,4,2688]{2,1,0:T(4,128)(2,1)S(1)} all-to-all(bf16[8,4,2688]{2,1,0:T(4,128)(2,1)S(1)} %fold.1), channel_id=1, replica_groups=mesh['dp'=4,'kz'=8,'ky'=4,'tp'=2] {'kz'}, dimensions={0} | all-to-all | bytes 344064 | tf_op jit(solution)/shard_map/all_to_all | solution.py:416
  35.1 0.4 chain.1
  35.5 13.6 %all_to_all.17 = bf16[32,4,1024]{2,1,0:T(4,128)(2,1)S(1)} all-to-all(bf16[32,4,1024]{2,1,0:T(4,128)(2,1)S(1)} %get-tuple-element.32), channel_id=1, replica_groups=mesh['dp'=4,'kz'=8,'ky'=4,'tp'=2] {'kz','ky'}, dimensions={0} | all-to-all | bytes 524288 | tf_op jit(solution)/shard_map/all_to_all | solution.py:418
  49.1 0.1 reshape.33.rows
  49.2 0.0 copy-done
  49.2 0.3 output.1.mine
  49.4 4.7 %collective-permute-start = (bf16[128,128]{1,0:T(8,128)(2,1)S(1)}, bf16[128,128]{1,0:T(8,128)(2,1)S(1)}, u32[]{:S(2)}, u32[]{:S(2)}) collective-permute-start(bf16[128,128]{1,0:T(8,128)(2,1)S(1)} %output.1.mine), channel_id=1, source_target_pairs={{0,1},{1,0},{2,3},{3,2},{4,5},{5,4},{6,7},{7,6},{8,9},{9,8},{10,11... | collective-permute-start | bytes 98312 | tf_op jit(solution)/shard_map/ppermute | solution.py:422
  54.1 2.5 %states.1 = (f32[1,5,16,64,128]{4,3,2,1,0:T(8,128)}, bf16[1,7,1024]{2,1,0:T(8,128)(2,1)}, bf16[1,7,256]{2,1,0:T(8,128)(2,1)}, bf16[1,7,256]{2,1,0:T(8,128)(2,1)}) custom-call(f32[1,16,64,128]{3,2,1,0:T(8,128)S(1)} %get-tuple-element.33.first, f32[8,1024]{1,0:T(8,128)S(1)} %get-tuple-element.34.moved, f32[4,256]{1,0:T(4,128)S(1)} %get-tuple-element.35.keys, ...), custom_call_target="tpu_custom_call" | custom-call | tf_op jit(solution)/shard_map/states/pallas_call | solution.py:316
  56.6 0.0 collective-permute-done.other
  56.6 0.8 %combine.1 = bf16[32,4,64]{2,1,0:T(4,128)(2,1)} custom-call(bf16[128,128]{1,0:T(8,128)(2,1)S(1)} %output.1.mine, bf16[128,128]{1,0:T(8,128)(2,1)S(1)} %collective-permute-done.other), custom_call_target="tpu_custom_call" | custom-call | tf_op jit(solution)/shard_map/combine/pallas_call | solution.py:371
Async XLA Ops:
  3.4 45.7 %copy-start = (bf16[1024,64]{0,1:T(8,128)(2,1)S(1)}, bf16[1024,64]{0,1:T(8,128)(2,1)}, u32[]{:S(2)}) copy-start(bf16[1024,64]{0,1:T(8,128)(2,1)} %param.32) | copy-start | bytes 393220
  49.4 7.1 %collective-permute-start = (bf16[128,128]{1,0:T(8,128)(2,1)S(1)}, bf16[128,128]{1,0:T(8,128)(2,1)S(1)}, u32[]{:S(2)}, u32[]{:S(2)}) collective-permute-start(bf16[128,128]{1,0:T(8,128)(2,1)S(1)} %output.1.mine), channel_id=1, source_target_pairs={{0,1},{1,0},{2,3},{3,2},{4,5},{5,4},{6,7},{7,6},{8,9},{9,8},{10,11... | collective-permute-start | bytes 98312 | tf_op jit(solution)/shard_map/ppermute | solution.py:422

commit v4 on v2

--- a/solution.py
+++ b/solution.py
@@ -34,13 +34,18 @@
     return high, x - high
 
 
-def project_kernel(tok, gain, wg, wv, wk, wq, ws, out, x_s, ws_s):
+def project_kernel(tok, gain, wg, wv, wk, wq, ws, *rest):
+    outs, (x_s, ws_s) = rest[:-2], rest[-2:]
+    near = len(outs)
     seqs, prop, _ = tok.shape
-    near, block, _ = out.shape
+    block = outs[0].shape[0]
     far = seqs // near
-    for i in range(seqs):
-        at = prop * ((i % near) * far + i // near)
-        x_s[at : at + prop, :] = tok[i].astype(F32)
+    here = lax.axis_index("ky")
+    for k in range(near):
+        place = lax.rem(here + k, near)
+        for z in range(far):
+            at = prop * (k * far + z)
+            x_s[at : at + prop, :] = tok[z * near + place].astype(F32)
     ws_s[...] = jnp.zeros(ws_s.shape, BF16)
     ws_s[: ws.shape[0], :] = ws[...]
     x = x_s[...]
@@ -50,8 +55,8 @@
     def put(at, product):
         width = product.shape[1]
         rounded = product.astype(BF16)
-        for j in range(near):
-            out[j, :, at : at + width] = rounded[block * j : block * (j + 1)]
+        for k, out in enumerate(outs):
+            out[:, at : at + width] = rounded[block * k : block * (k + 1)]
 
     at = 0
     for w in (wg, wv, wk, wq):
@@ -74,37 +79,39 @@
     columns = sum(w.shape[1] for w in weights[:4]) + LANES
     return pl.pallas_call(
         project_kernel,
-        out_specs=pl.BlockSpec(memory_space=VMEM),
-        out_shape=VMEM((near, seqs // near * prop, columns), BF16),
+        out_specs=[pl.BlockSpec(memory_space=VMEM)] * near,
+        out_shape=[VMEM((seqs // near * prop, columns), BF16)] * near,
         scratch_shapes=[VMEM((seqs * prop, feat), F32), VMEM((LANES, feat), BF16)],
         name="project",
     )(tokens, gain.reshape(1, feat), *weights[:4], weights[4].T)
 
 
-def fold_kernel(heads, arrived, out):
-    near, _, columns = arrived.shape
-    far, prop, _ = out.shape
+def fold_kernel(heads, order, *refs):
+    *arrived, out = refs
+    _, columns = arrived[0].shape
+    _, prop, _ = out.shape
     for at in range(0, columns, LANES):
-        total = arrived[0, :, at : at + LANES].astype(F32)
-        for j in range(1, near):
-            total = total + arrived[j, :, at : at + LANES].astype(F32)
+        total = arrived[0][:, at : at + LANES].astype(F32)
+        for block in arrived[1:]:
+            total = total + block[:, at : at + LANES].astype(F32)
         if at == columns - LANES:
             squares = total[:, heads : heads + 1] + total[:, heads + 1 : heads + 2]
             total = with_squares(total, squares, heads)
-        for k in range(far):
-            out[k, :, at : at + LANES] = total[prop * k : prop * (k + 1)].astype(BF16)
-
-
-def fold(arrived, far, heads):
-    _, rows, columns = arrived.shape
+        for k, place in enumerate(order):
+            out[k, :, at : at + LANES] = total[prop * place : prop * (place + 1)].astype(BF16)
+
+
+def fold(arrived, order, heads):
+    rows, columns = arrived[0].shape
+    far = len(order)
     vmem = pl.BlockSpec(memory_space=VMEM)
     return pl.pallas_call(
-        functools.partial(fold_kernel, heads),
-        in_specs=[vmem],
+        functools.partial(fold_kernel, heads, order),
+        in_specs=[vmem] * len(arrived),
         out_specs=vmem,
         out_shape=VMEM((far, rows // far, columns), BF16),
         name="fold",
-    )(local(arrived))
+    )(*map(local, arrived))
 
 
 def prepare_kernel(
@@ -369,21 +376,22 @@
     )(local(rows), local(w_out.T), local(gain))
 
 
-def combine_kernel(mine, other, out):
-    seqs, prop, features = out.shape
+def combine_kernel(order, mine, other, out):
+    _, prop, features = out.shape
     a, b = mine[...].astype(F32), other[...].astype(F32)
     squares_a = a[:, features : features + 1] + a[:, features + 1 : features + 2]
     squares_b = b[:, features : features + 1] + b[:, features + 1 : features + 2]
     scale = lax.rsqrt((squares_a + squares_b) / WIDTH + EPS)
     mixed = (a[:, :features] + b[:, :features]) * scale
-    for i in range(seqs):
-        out[i] = mixed[prop * i : prop * (i + 1)].astype(BF16)
-
-
-def combine(mine, other, seqs, features):
+    for i, seq in enumerate(order):
+        out[seq] = mixed[prop * i : prop * (i + 1)].astype(BF16)
+
+
+def combine(mine, other, order, features):
+    seqs = len(order)
     vmem = pl.BlockSpec(memory_space=VMEM)
     return pl.pallas_call(
-        combine_kernel,
+        functools.partial(combine_kernel, order),
         in_specs=[vmem, vmem],
         out_shape=jax.ShapeDtypeStruct((seqs, mine.shape[0] // seqs, features), BF16),
         name="combine",
@@ -412,9 +420,15 @@
     accepted,
 ):
     group_seqs, proposals, features = tokens.shape
+    near, far = lax.axis_size("ky"), lax.axis_size("kz")
+    near_order = [(near // 2 + i) % near for i in range(near)]
+    far_order = [(far // 2 + i) % far for i in range(far)]
+    order = [z * near + y for z in far_order for y in near_order]
     weights = (w_gate, w_value, w_key, w_query, w_step)
-    partial = project(tokens, in_gain, weights, lax.axis_size("ky"))
-    nearby = lax.all_to_all(partial, "ky", 0, 0, tiled=True)
+    own, *others = project(tokens, in_gain, weights, near)
+    nearby = {0: own}
+    for k in sorted(range(1, near), key=lambda k: -min(k, near - k)):
+        nearby[k] = lax.ppermute(others[k - 1], "ky", [(i, (i + k) % near) for i in range(near)])
     first, high, low, rows, base, taps, bias, rate, gain = prepare(
         accepted,
         past_states,
@@ -424,14 +438,14 @@
         decay_log,
         out_gain,
     )
-    partial = fold(nearby, lax.axis_size("kz"), w_step.shape[1])
-    arrived = lax.all_to_all(partial, "kz", 0, 0, tiled=True)
+    partial = fold([nearby[k] for k in range(near)], far_order, w_step.shape[1])
+    arrived = lax.all_to_all(partial, "kz", 0, 0, axis_index_groups=[far_order], tiled=True)
     sent, moved, keys, decay, new = chain(group_seqs, arrived, high, low, base, taps, bias, rate, gain)
-    gathered = lax.all_to_all(sent, KV, 0, 0, tiled=True)
+    gathered = lax.all_to_all(sent, KV, 0, 0, axis_index_groups=[order], tiled=True)
     saved = next_states(past_states.shape[1], first, moved, keys, decay, rows, new)
     mine = output(gathered.reshape(group_seqs * proposals, -1), w_out, gain)
     swap = [(i, 1 - i) for i in range(2)]
-    mixed = combine(mine, lax.ppermute(mine, "tp", swap), group_seqs, features)
+    mixed = combine(mine, lax.ppermute(mine, "tp", swap), order, features)
     return (mixed, *saved)
 
 

time: 57.2 us -> 51.5 us (0.900)
  blocking collectives: 28.4 us -> 16 us
  starting transfers between devices: 13 us -> 18.3 us
  waiting for transfers between devices: 5.86 us -> 7.34 us
    all_to_all x2 -> x1, blocking collectives: 28.4 us -> 16 us  [per_device(): lax.all_to_all(sent, KV, 0, 0, axis_index_groups=[order], tiled=True)]
    ppermute x1 -> x4, waiting for transfers between devices: 0.01 us -> 6.42 us  [the longest x3 6.41 us: per_device(): lax.ppermute(others[k - 1], 'ky', [(i, (i + k) % near) for i in range(nea...]
    all_to_all x1, waiting for transfers between devices: 5.85 us -> 0.92 us  [per_device(): lax.all_to_all(partial, 'kz', 0, 0, axis_index_groups=[far_order], tiled=...]
    ppermute x1 -> x4, starting transfers between devices: 4.66 us -> 7.92 us  [the longest x3 5.88 us: per_device(): lax.ppermute(others[k - 1], 'ky', [(i, (i + k) % near) for i in range(nea...]
    all_to_all x1, starting transfers between devices: 8.31 us -> 10.3 us  [per_device(): lax.all_to_all(partial, 'kz', 0, 0, axis_index_groups=[far_order], tiled=...]
  transfers between devices with their start and end apart: 2 -> 5, of which waited for: 1 -> 3; matrix products, arithmetic and copies ran while one was open for 0% -> 0% of each run, Pallas kernels for 8% -> 9%
where the time goes in v4:
time: 51.5 us; the launch traced here: 51.2 us
  starting transfers between devices  18.3 us (36%)
  blocking collectives  16 us (31%)
  Pallas kernels  8.12 us (16%)
  waiting for transfers between devices  7.34 us (14%)
  between operations  1.35 us (3%)
    all_to_all x1, blocking collectives, per_device(): lax.all_to_all(sent, KV, 0, 0, axis_index_groups=[order], tiled=True)  16 us
    all_to_all x1, starting transfers between devices, per_device(): lax.all_to_all(partial, 'kz', 0, 0, axis_index_groups=[far_order], tiled=...  10.3 us
    ppermute x3, waiting for transfers between devices, per_device(): lax.ppermute(others[k - 1], 'ky', [(i, (i + k) % near) for i in range(nea...  6.41 us
    ppermute x3, starting transfers between devices, per_device(): lax.ppermute(others[k - 1], 'ky', [(i, (i + k) % near) for i in range(nea...  5.88 us
    pallas_call x1, Pallas kernels, next_states(): pl.pallas_call(states_kernel, in_specs=[vmem] * 6, out_specs=[pl.BlockSpe...  2.47 us
    ppermute x1, starting transfers between devices, per_device(): mixed = combine(mine, lax.ppermute(mine, 'tp', swap), order, features)  2.04 us
    pallas_call x1, Pallas kernels, prepare(): pl.pallas_call(prepare_kernel, in_specs=[pl.BlockSpec(memory_space=pltpu....  1.96 us
    pallas_call x1, Pallas kernels, project(): pl.pallas_call(project_kernel, out_specs=[pl.BlockSpec(memory_space=VMEM)...  1.36 us
  transfers between devices with their start and end apart: 5, of which 3 were waited for; matrix products, arithmetic and copies ran while one was open for 0% of the time, Pallas kernels for 9%

profile of v4, /device:TPU:1, one launch (start us, length us, event | category | flops | bytes accessed | tf_op | source)
XLA Modules:
  0.0 51.2 jit_solution(4137515397401146111)
XLA Ops:
  0.6 1.4 %project.1 = (bf16[32,2688]{1,0:T(8,128)(2,1)S(1)}, bf16[32,2688]{1,0:T(8,128)(2,1)S(1)}, bf16[32,2688]{1,0:T(8,128)(2,1)S(1)}, bf16[32,2688]{1,0:T(8,128)(2,1)S(1)}) custom-call(bf16[32,4,64]{2,1,0:T(4,128)(2,1)} %tok.1, f32[1,64]{1,0:T(1,128)} %bitcast.9, bf16[64,1024]{1,0:T(8,128)(2,1)} %wg.1, bf16[64,1024]{1,0:T(8,128)(2,1)} %wv.1, bf16[64,256]{1,0:T(8,128)(2,1)} %wk.1, ...), custom_call_target="tpu_custom_call" | custom-call | tf_op jit(solution)/shard_map/project/pallas_call | solution.py:80
  2.0 2.2 %collective-permute-start = (bf16[32,2688]{1,0:T(8,128)(2,1)S(1)}, bf16[32,2688]{1,0:T(8,128)(2,1)S(1)}, u32[]{:S(2)}, u32[]{:S(2)}) collective-permute-start(bf16[32,2688]{1,0:T(8,128)(2,1)S(1)} %get-tuple-element.28), channel_id=1, source_target_pairs={{0,2},{2,4},{4,6},{6,0},{1,3},{3,5},{5,7},{7,1},{8,10},{10,12},{12... | collective-permute-start | bytes 516104 | tf_op jit(solution)/shard_map/ppermute | solution.py:431
  4.2 2.6 %collective-permute-start.1 = (bf16[32,2688]{1,0:T(8,128)(2,1)S(1)}, bf16[32,2688]{1,0:T(8,128)(2,1)S(1)}, u32[]{:S(2)}, u32[]{:S(2)}) collective-permute-start(bf16[32,2688]{1,0:T(8,128)(2,1)S(1)} %get-tuple-element.29), channel_id=1, source_target_pairs={{0,4},{2,6},{4,0},{6,2},{1,5},{3,7},{5,1},{7,3},{8,12},{10,14},{12... | collective-permute-start | bytes 516104 | tf_op jit(solution)/shard_map/ppermute | solution.py:431
  6.8 1.1 %collective-permute-start.2 = (bf16[32,2688]{1,0:T(8,128)(2,1)S(1)}, bf16[32,2688]{1,0:T(8,128)(2,1)S(1)}, u32[]{:S(2)}, u32[]{:S(2)}) collective-permute-start(bf16[32,2688]{1,0:T(8,128)(2,1)S(1)} %get-tuple-element.30), channel_id=1, source_target_pairs={{0,6},{2,0},{4,2},{6,4},{1,7},{3,1},{5,3},{7,5},{8,14},{10,8},{12,... | collective-permute-start | bytes 516104 | tf_op jit(solution)/shard_map/ppermute | solution.py:431
  7.9 0.5 %collective-permute-done.refs_1_ = bf16[32,2688]{1,0:T(8,128)(2,1)S(1)} collective-permute-done((bf16[32,2688]{1,0:T(8,128)(2,1)S(1)}, bf16[32,2688]{1,0:T(8,128)(2,1)S(1)}, u32[]{:S(2)}, u32[]{:S(2)}) %collective-permute-start) | collective-permute-done | bytes 172064 | tf_op jit(solution)/shard_map/ppermute | solution.py:431
  8.4 5.9 %collective-permute-done.1.refs_2_ = bf16[32,2688]{1,0:T(8,128)(2,1)S(1)} collective-permute-done((bf16[32,2688]{1,0:T(8,128)(2,1)S(1)}, bf16[32,2688]{1,0:T(8,128)(2,1)S(1)}, u32[]{:S(2)}, u32[]{:S(2)}) %collective-permute-start.1) | collective-permute-done | bytes 172064 | tf_op jit(solution)/shard_map/ppermute | solution.py:431
  14.3 0.0 collective-permute-done.2.refs_3_
  14.3 0.9 %fold.1 = bf16[8,4,2688]{2,1,0:T(4,128)(2,1)} custom-call(bf16[32,2688]{1,0:T(8,128)(2,1)S(1)} %get-tuple-element.27.refs_0_, bf16[32,2688]{1,0:T(8,128)(2,1)S(1)} %collective-permute-done.refs_1_, bf16[32,2688]{1,0:T(8,128)(2,1)S(1)} %collective-permute-done.1.refs_2_, bf16[32,2688]{1,0:T(8,128)(2,1)S(1)} %collective-permute-done.2.refs_3_), custom_call_target="tpu_custom_call" | custom-call | tf_op jit(solution)/shard_map/fold/pallas_call | solution.py:108
  15.2 0.0 copy-start
  15.2 10.3 %all-to-all-start = ((bf16[8,4,2688]{2,1,0:T(4,128)(2,1)}), bf16[8,4,2688]{2,1,0:T(4,128)(2,1)S(1)}, u32[]{:S(2)}, u32[]{:S(2)}) async-start(bf16[8,4,2688]{2,1,0:T(4,128)(2,1)} %fold.1), calls=%async_computation | async-start | bytes 344064 | tf_op jit(solution)/shard_map/all_to_all | solution.py:442
  26.2 2.0 %prepare.1 = (f32[1,16,64,128]{3,2,1,0:T(8,128)S(1)}, bf16[1024,128]{1,0:T(8,128)(2,1)S(1)}, bf16[1024,128]{1,0:T(8,128)(2,1)S(1)}, f32[3,1536]{1,0:T(4,128)S(1)...) custom-call(s32[1]{0:T(128)S(6)} %copy.24.accepted, ...), custom_call_target="tpu_custom_call" | custom-call | tf_op jit(solution)/shard_map/prepare/pallas_call | solution.py:178
  28.1 0.9 %all-to-all-done.arrived = bf16[8,4,2688]{2,1,0:T(4,128)(2,1)S(1)} async-done(((bf16[8,4,2688]{2,1,0:T(4,128)(2,1)}), bf16[8,4,2688]{2,1,0:T(4,128)(2,1)S(1)}, u32[]{:S(2)}, u32[]{:S(2)}) %all-to-all-start) | async-done | bytes 172064 | tf_op jit(solution)/shard_map/all_to_all | solution.py:442
  29.0 0.4 chain.1
  29.5 16.0 %all_to_all.10 = bf16[32,4,1024]{2,1,0:T(4,128)(2,1)S(1)} all-to-all(bf16[32,4,1024]{2,1,0:T(4,128)(2,1)S(1)} %get-tuple-element.38), channel_id=1, replica_groups={{36,38,32,34,44,46,40,42,52,54,48,50,60,62,56,58,4,6,0,2,12,14,8,10,20,..., dimensions={0} | all-to-all | bytes 524288 | tf_op jit(solution)/shard_map/all_to_all | solution.py:444
  45.5 0.1 reshape.29.rows
  45.6 0.0 copy-done
  45.6 0.3 output.1.mine
  45.9 2.0 %collective-permute-start.3 = (bf16[128,128]{1,0:T(8,128)(2,1)S(1)}, bf16[128,128]{1,0:T(8,128)(2,1)S(1)}, u32[]{:S(2)}, u32[]{:S(2)}) collective-permute-start(bf16[128,128]{1,0:T(8,128)(2,1)S(1)} %output.1.mine), channel_id=1, source_target_pairs={{0,1},{1,0},{2,3},{3,2},{4,5},{5,4},{6,7},{7,6},{8,9},{9,8},{10,11... | collective-permute-start | bytes 98312 | tf_op jit(solution)/shard_map/ppermute | solution.py:448
  47.9 2.5 %states.3 = (f32[1,5,16,64,128]{4,3,2,1,0:T(8,128)}, bf16[1,7,1024]{2,1,0:T(8,128)(2,1)}, bf16[1,7,256]{2,1,0:T(8,128)(2,1)}, bf16[1,7,256]{2,1,0:T(8,128)(2,1)}) custom-call(f32[1,16,64,128]{3,2,1,0:T(8,128)S(1)} %get-tuple-element.39.first, f32[8,1024]{1,0:T(8,128)S(1)} %get-tuple-element.40.moved, f32[4,256]{1,0:T(4,128)S(1)} %get-tuple-element.41.keys, ...), custom_call_target="tpu_custom_call" | custom-call | tf_op jit(solution)/shard_map/states/pallas_call | solution.py:337
  50.4 0.0 collective-permute-done.3.other
  50.4 0.8 %combine.1 = bf16[32,4,64]{2,1,0:T(4,128)(2,1)} custom-call(bf16[128,128]{1,0:T(8,128)(2,1)S(1)} %output.1.mine, bf16[128,128]{1,0:T(8,128)(2,1)S(1)} %collective-permute-done.3.other), custom_call_target="tpu_custom_call" | custom-call | tf_op jit(solution)/shard_map/combine/pallas_call | solution.py:393
Async XLA Ops:
  2.0 6.4 %collective-permute-start = (bf16[32,2688]{1,0:T(8,128)(2,1)S(1)}, bf16[32,2688]{1,0:T(8,128)(2,1)S(1)}, u32[]{:S(2)}, u32[]{:S(2)}) collective-permute-start(bf16[32,2688]{1,0:T(8,128)(2,1)S(1)} %get-tuple-element.28), channel_id=1, source_target_pairs={{0,2},{2,4},{4,6},{6,0},{1,3},{3,5},{5,7},{7,1},{8,10},{10,12},{12... | collective-permute-start | bytes 516104 | tf_op jit(solution)/shard_map/ppermute | solution.py:431
  4.2 10.1 %collective-permute-start.1 = (bf16[32,2688]{1,0:T(8,128)(2,1)S(1)}, bf16[32,2688]{1,0:T(8,128)(2,1)S(1)}, u32[]{:S(2)}, u32[]{:S(2)}) collective-permute-start(bf16[32,2688]{1,0:T(8,128)(2,1)S(1)} %get-tuple-element.29), channel_id=1, source_target_pairs={{0,4},{2,6},{4,0},{6,2},{1,5},{3,7},{5,1},{7,3},{8,12},{10,14},{12... | collective-permute-start | bytes 516104 | tf_op jit(solution)/shard_map/ppermute | solution.py:431
  6.8 7.5 %collective-permute-start.2 = (bf16[32,2688]{1,0:T(8,128)(2,1)S(1)}, bf16[32,2688]{1,0:T(8,128)(2,1)S(1)}, u32[]{:S(2)}, u32[]{:S(2)}) collective-permute-start(bf16[32,2688]{1,0:T(8,128)(2,1)S(1)} %get-tuple-element.30), channel_id=1, source_target_pairs={{0,6},{2,0},{4,2},{6,4},{1,7},{3,1},{5,3},{7,5},{8,14},{10,8},{12,... | collective-permute-start | bytes 516104 | tf_op jit(solution)/shard_map/ppermute | solution.py:431
  15.2 30.4 %copy-start = (bf16[1024,64]{0,1:T(8,128)(2,1)S(1)}, bf16[1024,64]{0,1:T(8,128)(2,1)}, u32[]{:S(2)}) copy-start(bf16[1024,64]{0,1:T(8,128)(2,1)} %param.32) | copy-start | bytes 393220
  15.2 13.9 %all-to-all-start = ((bf16[8,4,2688]{2,1,0:T(4,128)(2,1)}), bf16[8,4,2688]{2,1,0:T(4,128)(2,1)S(1)}, u32[]{:S(2)}, u32[]{:S(2)}) async-start(bf16[8,4,2688]{2,1,0:T(4,128)(2,1)} %fold.1), calls=%async_computation | async-start | bytes 344064 | tf_op jit(solution)/shard_map/all_to_all | solution.py:442
  45.9 4.5 %collective-permute-start.3 = (bf16[128,128]{1,0:T(8,128)(2,1)S(1)}, bf16[128,128]{1,0:T(8,128)(2,1)S(1)}, u32[]{:S(2)}, u32[]{:S(2)}) collective-permute-start(bf16[128,128]{1,0:T(8,128)(2,1)S(1)} %output.1.mine), channel_id=1, source_target_pairs={{0,1},{1,0},{2,3},{3,2},{4,5},{5,4},{6,7},{7,6},{8,9},{9,8},{10,11... | collective-permute-start | bytes 98312 | tf_op jit(solution)/shard_map/ppermute | solution.py:448

commit v5 on v4

--- a/solution.py
+++ b/solution.py
@@ -421,9 +421,8 @@
 ):
     group_seqs, proposals, features = tokens.shape
     near, far = lax.axis_size("ky"), lax.axis_size("kz")
-    near_order = [(near // 2 + i) % near for i in range(near)]
-    far_order = [(far // 2 + i) % far for i in range(far)]
-    order = [z * near + y for z in far_order for y in near_order]
+    far_order = [(far // 2 + 1 + i) % far for i in range(far)]
+    order = [(far // 2 + i) % far * near + (near // 2 + j) % near for i in range(far) for j in range(near)]
     weights = (w_gate, w_value, w_key, w_query, w_step)
     own, *others = project(tokens, in_gain, weights, near)
     nearby = {0: own}

time: 51.5 us -> 51.8 us (level)
  waiting for transfers between devices: 7.34 us -> 8.06 us
  blocking collectives: 16 us -> 15.4 us
    all_to_all x1, waiting for transfers between devices: 0.92 us -> 1.65 us  [per_device(): lax.all_to_all(partial, 'kz', 0, 0, axis_index_groups=[far_order], tiled=...]
    all_to_all x1, blocking collectives: 16 us -> 15.4 us  [per_device(): lax.all_to_all(sent, KV, 0, 0, axis_index_groups=[order], tiled=True)]
    ppermute x1, starting transfers between devices: 2.04 us -> 2.62 us  [per_device(): mixed = combine(mine, lax.ppermute(mine, 'tp', swap), order, features)]
where the time goes in v5:
time: 51.8 us; the launch traced here: 51.4 us
  starting transfers between devices  18.4 us (36%)
  blocking collectives  15.4 us (30%)
  Pallas kernels  8.12 us (16%)
  waiting for transfers between devices  8.06 us (16%)
  between operations  1.35 us (3%)
    all_to_all x1, blocking collectives, per_device(): lax.all_to_all(sent, KV, 0, 0, axis_index_groups=[order], tiled=True)  15.4 us
    all_to_all x1, starting transfers between devices, per_device(): lax.all_to_all(partial, 'kz', 0, 0, axis_index_groups=[far_order], tiled=...  9.9 us
    ppermute x3, waiting for transfers between devices, per_device(): lax.ppermute(others[k - 1], 'ky', [(i, (i + k) % near) for i in range(nea...  6.41 us
    ppermute x3, starting transfers between devices, per_device(): lax.ppermute(others[k - 1], 'ky', [(i, (i + k) % near) for i in range(nea...  5.88 us
    ppermute x1, starting transfers between devices, per_device(): mixed = combine(mine, lax.ppermute(mine, 'tp', swap), order, features)  2.62 us
    pallas_call x1, Pallas kernels, next_states(): pl.pallas_call(states_kernel, in_specs=[vmem] * 6, out_specs=[pl.BlockSpe...  2.47 us
    pallas_call x1, Pallas kernels, prepare(): pl.pallas_call(prepare_kernel, in_specs=[pl.BlockSpec(memory_space=pltpu....  1.96 us
    all_to_all x1, waiting for transfers between devices, per_device(): lax.all_to_all(partial, 'kz', 0, 0, axis_index_groups=[far_order], tiled=...  1.65 us
  transfers between devices with their start and end apart: 5, of which 3 were waited for; matrix products, arithmetic and copies ran while one was open for 0% of the time, Pallas kernels for 9%

profile of v5, /device:TPU:1, one launch (start us, length us, event | category | flops | bytes accessed | tf_op | source)
XLA Modules:
  0.0 51.4 jit_solution(8568756133752737466)
XLA Ops:
  0.6 1.4 %project.1 = (bf16[32,2688]{1,0:T(8,128)(2,1)S(1)}, bf16[32,2688]{1,0:T(8,128)(2,1)S(1)}, bf16[32,2688]{1,0:T(8,128)(2,1)S(1)}, bf16[32,2688]{1,0:T(8,128)(2,1)S(1)}) custom-call(bf16[32,4,64]{2,1,0:T(4,128)(2,1)} %tok.1, f32[1,64]{1,0:T(1,128)} %bitcast.9, bf16[64,1024]{1,0:T(8,128)(2,1)} %wg.1, bf16[64,1024]{1,0:T(8,128)(2,1)} %wv.1, bf16[64,256]{1,0:T(8,128)(2,1)} %wk.1, ...), custom_call_target="tpu_custom_call" | custom-call | tf_op jit(solution)/shard_map/project/pallas_call | solution.py:80
  2.0 2.2 %collective-permute-start = (bf16[32,2688]{1,0:T(8,128)(2,1)S(1)}, bf16[32,2688]{1,0:T(8,128)(2,1)S(1)}, u32[]{:S(2)}, u32[]{:S(2)}) collective-permute-start(bf16[32,2688]{1,0:T(8,128)(2,1)S(1)} %get-tuple-element.28), channel_id=1, source_target_pairs={{0,2},{2,4},{4,6},{6,0},{1,3},{3,5},{5,7},{7,1},{8,10},{10,12},{12... | collective-permute-start | bytes 516104 | tf_op jit(solution)/shard_map/ppermute | solution.py:430
  4.2 2.6 %collective-permute-start.1 = (bf16[32,2688]{1,0:T(8,128)(2,1)S(1)}, bf16[32,2688]{1,0:T(8,128)(2,1)S(1)}, u32[]{:S(2)}, u32[]{:S(2)}) collective-permute-start(bf16[32,2688]{1,0:T(8,128)(2,1)S(1)} %get-tuple-element.29), channel_id=1, source_target_pairs={{0,4},{2,6},{4,0},{6,2},{1,5},{3,7},{5,1},{7,3},{8,12},{10,14},{12... | collective-permute-start | bytes 516104 | tf_op jit(solution)/shard_map/ppermute | solution.py:430
  6.8 1.1 %collective-permute-start.2 = (bf16[32,2688]{1,0:T(8,128)(2,1)S(1)}, bf16[32,2688]{1,0:T(8,128)(2,1)S(1)}, u32[]{:S(2)}, u32[]{:S(2)}) collective-permute-start(bf16[32,2688]{1,0:T(8,128)(2,1)S(1)} %get-tuple-element.30), channel_id=1, source_target_pairs={{0,6},{2,0},{4,2},{6,4},{1,7},{3,1},{5,3},{7,5},{8,14},{10,8},{12,... | collective-permute-start | bytes 516104 | tf_op jit(solution)/shard_map/ppermute | solution.py:430
  7.9 0.5 %collective-permute-done.refs_1_ = bf16[32,2688]{1,0:T(8,128)(2,1)S(1)} collective-permute-done((bf16[32,2688]{1,0:T(8,128)(2,1)S(1)}, bf16[32,2688]{1,0:T(8,128)(2,1)S(1)}, u32[]{:S(2)}, u32[]{:S(2)}) %collective-permute-start) | collective-permute-done | bytes 172064 | tf_op jit(solution)/shard_map/ppermute | solution.py:430
  8.4 5.9 %collective-permute-done.1.refs_2_ = bf16[32,2688]{1,0:T(8,128)(2,1)S(1)} collective-permute-done((bf16[32,2688]{1,0:T(8,128)(2,1)S(1)}, bf16[32,2688]{1,0:T(8,128)(2,1)S(1)}, u32[]{:S(2)}, u32[]{:S(2)}) %collective-permute-start.1) | collective-permute-done | bytes 172064 | tf_op jit(solution)/shard_map/ppermute | solution.py:430
  14.3 0.0 collective-permute-done.2.refs_3_
  14.3 0.9 %fold.1 = bf16[8,4,2688]{2,1,0:T(4,128)(2,1)} custom-call(bf16[32,2688]{1,0:T(8,128)(2,1)S(1)} %get-tuple-element.27.refs_0_, bf16[32,2688]{1,0:T(8,128)(2,1)S(1)} %collective-permute-done.refs_1_, bf16[32,2688]{1,0:T(8,128)(2,1)S(1)} %collective-permute-done.1.refs_2_, bf16[32,2688]{1,0:T(8,128)(2,1)S(1)} %collective-permute-done.2.refs_3_), custom_call_target="tpu_custom_call" | custom-call | tf_op jit(solution)/shard_map/fold/pallas_call | solution.py:108
  15.2 0.0 copy-start
  15.2 9.9 %all-to-all-start = ((bf16[8,4,2688]{2,1,0:T(4,128)(2,1)}), bf16[8,4,2688]{2,1,0:T(4,128)(2,1)S(1)}, u32[]{:S(2)}, u32[]{:S(2)}) async-start(bf16[8,4,2688]{2,1,0:T(4,128)(2,1)} %fold.1), calls=%async_computation | async-start | bytes 344064 | tf_op jit(solution)/shard_map/all_to_all | solution.py:441
  25.7 2.0 %prepare.1 = (f32[1,16,64,128]{3,2,1,0:T(8,128)S(1)}, bf16[1024,128]{1,0:T(8,128)(2,1)S(1)}, bf16[1024,128]{1,0:T(8,128)(2,1)S(1)}, f32[3,1536]{1,0:T(4,128)S(1)...) custom-call(s32[1]{0:T(128)S(6)} %copy.24.accepted, ...), custom_call_target="tpu_custom_call" | custom-call | tf_op jit(solution)/shard_map/prepare/pallas_call | solution.py:178
  27.7 1.6 %all-to-all-done.arrived = bf16[8,4,2688]{2,1,0:T(4,128)(2,1)S(1)} async-done(((bf16[8,4,2688]{2,1,0:T(4,128)(2,1)}), bf16[8,4,2688]{2,1,0:T(4,128)(2,1)S(1)}, u32[]{:S(2)}, u32[]{:S(2)}) %all-to-all-start) | async-done | bytes 172064 | tf_op jit(solution)/shard_map/all_to_all | solution.py:441
  29.3 0.4 chain.1
  29.8 15.4 %all_to_all.10 = bf16[32,4,1024]{2,1,0:T(4,128)(2,1)S(1)} all-to-all(bf16[32,4,1024]{2,1,0:T(4,128)(2,1)S(1)} %get-tuple-element.38), channel_id=1, replica_groups={{36,38,32,34,44,46,40,42,52,54,48,50,60,62,56,58,4,6,0,2,12,14,8,10,20,..., dimensions={0} | all-to-all | bytes 524288 | tf_op jit(solution)/shard_map/all_to_all | solution.py:443
  45.2 0.1 reshape.29.rows
  45.2 0.0 copy-done
  45.2 0.3 output.1.mine
  45.5 2.6 %collective-permute-start.3 = (bf16[128,128]{1,0:T(8,128)(2,1)S(1)}, bf16[128,128]{1,0:T(8,128)(2,1)S(1)}, u32[]{:S(2)}, u32[]{:S(2)}) collective-permute-start(bf16[128,128]{1,0:T(8,128)(2,1)S(1)} %output.1.mine), channel_id=1, source_target_pairs={{0,1},{1,0},{2,3},{3,2},{4,5},{5,4},{6,7},{7,6},{8,9},{9,8},{10,11... | collective-permute-start | bytes 98312 | tf_op jit(solution)/shard_map/ppermute | solution.py:447
  48.1 2.5 %states.3 = (f32[1,5,16,64,128]{4,3,2,1,0:T(8,128)}, bf16[1,7,1024]{2,1,0:T(8,128)(2,1)}, bf16[1,7,256]{2,1,0:T(8,128)(2,1)}, bf16[1,7,256]{2,1,0:T(8,128)(2,1)}) custom-call(f32[1,16,64,128]{3,2,1,0:T(8,128)S(1)} %get-tuple-element.39.first, f32[8,1024]{1,0:T(8,128)S(1)} %get-tuple-element.40.moved, f32[4,256]{1,0:T(4,128)S(1)} %get-tuple-element.41.keys, ...), custom_call_target="tpu_custom_call" | custom-call | tf_op jit(solution)/shard_map/states/pallas_call | solution.py:337
  50.6 0.0 collective-permute-done.3.other
  50.6 0.8 %combine.1 = bf16[32,4,64]{2,1,0:T(4,128)(2,1)} custom-call(bf16[128,128]{1,0:T(8,128)(2,1)S(1)} %output.1.mine, bf16[128,128]{1,0:T(8,128)(2,1)S(1)} %collective-permute-done.3.other), custom_call_target="tpu_custom_call" | custom-call | tf_op jit(solution)/shard_map/combine/pallas_call | solution.py:393
Async XLA Ops:
  2.0 6.4 %collective-permute-start = (bf16[32,2688]{1,0:T(8,128)(2,1)S(1)}, bf16[32,2688]{1,0:T(8,128)(2,1)S(1)}, u32[]{:S(2)}, u32[]{:S(2)}) collective-permute-start(bf16[32,2688]{1,0:T(8,128)(2,1)S(1)} %get-tuple-element.28), channel_id=1, source_target_pairs={{0,2},{2,4},{4,6},{6,0},{1,3},{3,5},{5,7},{7,1},{8,10},{10,12},{12... | collective-permute-start | bytes 516104 | tf_op jit(solution)/shard_map/ppermute | solution.py:430
  4.2 10.1 %collective-permute-start.1 = (bf16[32,2688]{1,0:T(8,128)(2,1)S(1)}, bf16[32,2688]{1,0:T(8,128)(2,1)S(1)}, u32[]{:S(2)}, u32[]{:S(2)}) collective-permute-start(bf16[32,2688]{1,0:T(8,128)(2,1)S(1)} %get-tuple-element.29), channel_id=1, source_target_pairs={{0,4},{2,6},{4,0},{6,2},{1,5},{3,7},{5,1},{7,3},{8,12},{10,14},{12... | collective-permute-start | bytes 516104 | tf_op jit(solution)/shard_map/ppermute | solution.py:430
  6.8 7.5 %collective-permute-start.2 = (bf16[32,2688]{1,0:T(8,128)(2,1)S(1)}, bf16[32,2688]{1,0:T(8,128)(2,1)S(1)}, u32[]{:S(2)}, u32[]{:S(2)}) collective-permute-start(bf16[32,2688]{1,0:T(8,128)(2,1)S(1)} %get-tuple-element.30), channel_id=1, source_target_pairs={{0,6},{2,0},{4,2},{6,4},{1,7},{3,1},{5,3},{7,5},{8,14},{10,8},{12,... | collective-permute-start | bytes 516104 | tf_op jit(solution)/shard_map/ppermute | solution.py:430
  15.2 30.1 %copy-start = (bf16[1024,64]{0,1:T(8,128)(2,1)S(1)}, bf16[1024,64]{0,1:T(8,128)(2,1)}, u32[]{:S(2)}) copy-start(bf16[1024,64]{0,1:T(8,128)(2,1)} %param.32) | copy-start | bytes 393220
  15.2 14.2 %all-to-all-start = ((bf16[8,4,2688]{2,1,0:T(4,128)(2,1)}), bf16[8,4,2688]{2,1,0:T(4,128)(2,1)S(1)}, u32[]{:S(2)}, u32[]{:S(2)}) async-start(bf16[8,4,2688]{2,1,0:T(4,128)(2,1)} %fold.1), calls=%async_computation | async-start | bytes 344064 | tf_op jit(solution)/shard_map/all_to_all | solution.py:441
  45.5 5.1 %collective-permute-start.3 = (bf16[128,128]{1,0:T(8,128)(2,1)S(1)}, bf16[128,128]{1,0:T(8,128)(2,1)S(1)}, u32[]{:S(2)}, u32[]{:S(2)}) collective-permute-start(bf16[128,128]{1,0:T(8,128)(2,1)S(1)} %output.1.mine), channel_id=1, source_target_pairs={{0,1},{1,0},{2,3},{3,2},{4,5},{5,4},{6,7},{7,6},{8,9},{9,8},{10,11... | collective-permute-start | bytes 98312 | tf_op jit(solution)/shard_map/ppermute | solution.py:447

commit v6 on v5

--- a/solution.py
+++ b/solution.py
@@ -17,6 +17,7 @@
 F32 = jnp.float32
 BF16 = jnp.bfloat16
 LANES = 128
+PACK = 4
 VMEM = pltpu.VMEM
 NT = (((1,), (1,)), ((), ()))
 
@@ -38,8 +39,8 @@
     outs, (x_s, ws_s) = rest[:-2], rest[-2:]
     near = len(outs)
     seqs, prop, _ = tok.shape
-    block = outs[0].shape[0]
     far = seqs // near
+    block = far * prop
     here = lax.axis_index("ky")
     for k in range(near):
         place = lax.rem(here + k, near)
@@ -52,20 +53,21 @@
     squares = jnp.sum(x * x, axis=1, keepdims=True)
     normed = (x * gain[...]).astype(BF16)
 
-    def put(at, product):
-        width = product.shape[1]
-        rounded = product.astype(BF16)
-        for k, out in enumerate(outs):
-            out[:, at : at + width] = rounded[block * k : block * (k + 1)]
-
     at = 0
     for w in (wg, wv, wk, wq):
-        for c in range(0, w.shape[1], 256):
-            put(at, jnp.dot(normed, w[:, c : c + 256], preferred_element_type=F32))
-            at += 256
+        for c in range(0, w.shape[1], 2 * LANES):
+            product = jnp.dot(normed, w[:, c : c + 2 * LANES], preferred_element_type=F32).astype(BF16)
+            for part in (product[:, :LANES], product[:, LANES:]):
+                for k, out in enumerate(outs):
+                    out[at : at + block, :] = part[block * k : block * (k + 1)]
+                at += block
     heads = ws.shape[0]
     extra = lax.dot_general(normed, ws_s[...], NT, preferred_element_type=F32)
-    put(at, with_squares(extra, squares, heads))
+    extra = with_squares(extra, squares, heads)
+    strip, wide = block // PACK, LANES // PACK
+    for k, out in enumerate(outs):
+        strips = [extra[block * k + strip * j : block * k + strip * (j + 1), :wide] for j in range(PACK)]
+        out[at:, :] = jnp.concatenate(strips, axis=1).astype(BF16)
 
 
 def with_squares(extra, squares, at):
@@ -76,11 +78,12 @@
 
 def project(tokens, gain, weights, near):
     seqs, prop, feat = tokens.shape
-    columns = sum(w.shape[1] for w in weights[:4]) + LANES
+    block = seqs // near * prop
+    rows = sum(w.shape[1] for w in weights[:4]) // LANES * block + block // PACK
     return pl.pallas_call(
         project_kernel,
         out_specs=[pl.BlockSpec(memory_space=VMEM)] * near,
-        out_shape=[VMEM((seqs // near * prop, columns), BF16)] * near,
+        out_shape=[VMEM((rows, LANES), BF16)] * near,
         scratch_shapes=[VMEM((seqs * prop, feat), F32), VMEM((LANES, feat), BF16)],
         name="project",
     )(tokens, gain.reshape(1, feat), *weights[:4], weights[4].T)
@@ -88,28 +91,33 @@
 
 def fold_kernel(heads, order, *refs):
     *arrived, out = refs
-    _, columns = arrived[0].shape
-    _, prop, _ = out.shape
+    far, prop, columns = out.shape
+    block = far * prop
     for at in range(0, columns, LANES):
-        total = arrived[0][:, at : at + LANES].astype(F32)
-        for block in arrived[1:]:
-            total = total + block[:, at : at + LANES].astype(F32)
-        if at == columns - LANES:
+        start = at // LANES * block
+        last = at == columns - LANES
+        part = slice(start, start + (block // PACK if last else block))
+        total = arrived[0][part].astype(F32)
+        for other in arrived[1:]:
+            total = total + other[part].astype(F32)
+        if last:
+            wide = LANES // PACK
+            total = jnp.concatenate([total[:, wide * j : wide * (j + 1)] for j in range(PACK)], axis=0)
+            total = jnp.concatenate([total, jnp.zeros((block, LANES - wide), F32)], axis=1)
             squares = total[:, heads : heads + 1] + total[:, heads + 1 : heads + 2]
             total = with_squares(total, squares, heads)
         for k, place in enumerate(order):
             out[k, :, at : at + LANES] = total[prop * place : prop * (place + 1)].astype(BF16)
 
 
-def fold(arrived, order, heads):
-    rows, columns = arrived[0].shape
+def fold(arrived, order, prop, columns, heads):
     far = len(order)
     vmem = pl.BlockSpec(memory_space=VMEM)
     return pl.pallas_call(
         functools.partial(fold_kernel, heads, order),
         in_specs=[vmem] * len(arrived),
         out_specs=vmem,
-        out_shape=VMEM((far, rows // far, columns), BF16),
+        out_shape=VMEM((far, prop, columns), BF16),
         name="fold",
     )(*map(local, arrived))
 
@@ -424,6 +432,7 @@
     far_order = [(far // 2 + 1 + i) % far for i in range(far)]
     order = [(far // 2 + i) % far * near + (near // 2 + j) % near for i in range(far) for j in range(near)]
     weights = (w_gate, w_value, w_key, w_query, w_step)
+    columns = sum(w.shape[1] for w in weights[:4]) + LANES
     own, *others = project(tokens, in_gain, weights, near)
     nearby = {0: own}
     for k in sorted(range(1, near), key=lambda k: -min(k, near - k)):
@@ -437,7 +446,7 @@
         decay_log,
         out_gain,
     )
-    partial = fold([nearby[k] for k in range(near)], far_order, w_step.shape[1])
+    partial = fold([nearby[k] for k in range(near)], far_order, proposals, columns, w_step.shape[1])
     arrived = lax.all_to_all(partial, "kz", 0, 0, axis_index_groups=[far_order], tiled=True)
     sent, moved, keys, decay, new = chain(group_seqs, arrived, high, low, base, taps, bias, rate, gain)
     gathered = lax.all_to_all(sent, KV, 0, 0, axis_index_groups=[order], tiled=True)

time: 51.8 us -> 51.5 us (level)
  no operation moved by 1% of the time
where the time goes in v6:
time: 51.5 us; the launch traced here: 51.2 us
  starting transfers between devices  18.6 us (36%)
  blocking collectives  15.1 us (29%)
  Pallas kernels  8.26 us (16%)
  waiting for transfers between devices  7.79 us (15%)
  between operations  1.34 us (3%)
    all_to_all x1, blocking collectives, per_device(): lax.all_to_all(sent, KV, 0, 0, axis_index_groups=[order], tiled=True)  15.1 us
    all_to_all x1, starting transfers between devices, per_device(): lax.all_to_all(partial, 'kz', 0, 0, axis_index_groups=[far_order], tiled=...  9.9 us
    ppermute x3, waiting for transfers between devices, per_device(): lax.ppermute(others[k - 1], 'ky', [(i, (i + k) % near) for i in range(nea...  6.14 us
    ppermute x3, starting transfers between devices, per_device(): lax.ppermute(others[k - 1], 'ky', [(i, (i + k) % near) for i in range(nea...  5.88 us
    ppermute x1, starting transfers between devices, per_device(): mixed = combine(mine, lax.ppermute(mine, 'tp', swap), order, features)  2.83 us
    pallas_call x1, Pallas kernels, next_states(): pl.pallas_call(states_kernel, in_specs=[vmem] * 6, out_specs=[pl.BlockSpe...  2.47 us
    pallas_call x1, Pallas kernels, prepare(): pl.pallas_call(prepare_kernel, in_specs=[pl.BlockSpec(memory_space=pltpu....  1.96 us
    all_to_all x1, waiting for transfers between devices, per_device(): lax.all_to_all(partial, 'kz', 0, 0, axis_index_groups=[far_order], tiled=...  1.65 us
  transfers between devices with their start and end apart: 5, of which 3 were waited for; matrix products, arithmetic and copies ran while one was open for 0% of the time, Pallas kernels for 9%

profile of v6, /device:TPU:1, one launch (start us, length us, event | category | flops | bytes accessed | tf_op | source)
XLA Modules:
  0.0 51.2 jit_solution(3274348389102367168)
XLA Ops:
  0.6 1.4 %project.1 = (bf16[648,128]{1,0:T(8,128)(2,1)S(1)}, bf16[648,128]{1,0:T(8,128)(2,1)S(1)}, bf16[648,128]{1,0:T(8,128)(2,1)S(1)}, bf16[648,128]{1,0:T(8,128)(2,1)S(1)}) custom-call(bf16[32,4,64]{2,1,0:T(4,128)(2,1)} %tok.1, f32[1,64]{1,0:T(1,128)} %bitcast.9, bf16[64,1024]{1,0:T(8,128)(2,1)} %wg.1, bf16[64,1024]{1,0:T(8,128)(2,1)} %wv.1, bf16[64,256]{1,0:T(8,128)(2,1)} %wk.1, ...), custom_call_target="tpu_custom_call" | custom-call | tf_op jit(solution)/shard_map/project/pallas_call | solution.py:83
  2.1 2.2 %collective-permute-start = (bf16[648,128]{1,0:T(8,128)(2,1)S(1)}, bf16[648,128]{1,0:T(8,128)(2,1)S(1)}, u32[]{:S(2)}, u32[]{:S(2)}) collective-permute-start(bf16[648,128]{1,0:T(8,128)(2,1)S(1)} %get-tuple-element.28), channel_id=1, source_target_pairs={{0,2},{2,4},{4,6},{6,0},{1,3},{3,5},{5,7},{7,1},{8,10},{10,12},{12... | collective-permute-start | bytes 497672 | tf_op jit(solution)/shard_map/ppermute | solution.py:439
  4.3 2.6 %collective-permute-start.1 = (bf16[648,128]{1,0:T(8,128)(2,1)S(1)}, bf16[648,128]{1,0:T(8,128)(2,1)S(1)}, u32[]{:S(2)}, u32[]{:S(2)}) collective-permute-start(bf16[648,128]{1,0:T(8,128)(2,1)S(1)} %get-tuple-element.29), channel_id=1, source_target_pairs={{0,4},{2,6},{4,0},{6,2},{1,5},{3,7},{5,1},{7,3},{8,12},{10,14},{12... | collective-permute-start | bytes 497672 | tf_op jit(solution)/shard_map/ppermute | solution.py:439
  6.9 1.1 %collective-permute-start.2 = (bf16[648,128]{1,0:T(8,128)(2,1)S(1)}, bf16[648,128]{1,0:T(8,128)(2,1)S(1)}, u32[]{:S(2)}, u32[]{:S(2)}) collective-permute-start(bf16[648,128]{1,0:T(8,128)(2,1)S(1)} %get-tuple-element.30), channel_id=1, source_target_pairs={{0,6},{2,0},{4,2},{6,4},{1,7},{3,1},{5,3},{7,5},{8,14},{10,8},{12,... | collective-permute-start | bytes 497672 | tf_op jit(solution)/shard_map/ppermute | solution.py:439
  7.9 0.5 collective-permute-done.refs_1_
  8.4 5.7 %collective-permute-done.1.refs_2_ = bf16[648,128]{1,0:T(8,128)(2,1)S(1)} collective-permute-done((bf16[648,128]{1,0:T(8,128)(2,1)S(1)}, bf16[648,128]{1,0:T(8,128)(2,1)S(1)}, u32[]{:S(2)}, u32[]{:S(2)}) %collective-permute-start.1) | collective-permute-done | bytes 165920 | tf_op jit(solution)/shard_map/ppermute | solution.py:439
  14.1 0.0 collective-permute-done.2.refs_3_
  14.1 0.9 %fold.1 = bf16[8,4,2688]{2,1,0:T(4,128)(2,1)} custom-call(bf16[648,128]{1,0:T(8,128)(2,1)S(1)} %get-tuple-element.27.refs_0_, bf16[648,128]{1,0:T(8,128)(2,1)S(1)} %collective-permute-done.refs_1_, bf16[648,128]{1,0:T(8,128)(2,1)S(1)} %collective-permute-done.1.refs_2_, bf16[648,128]{1,0:T(8,128)(2,1)S(1)} %collective-permute-done.2.refs_3_), custom_call_target="tpu_custom_call" | custom-call | tf_op jit(solution)/shard_map/fold/pallas_call | solution.py:116
  15.0 0.0 copy-start
  15.0 9.9 %all-to-all-start = ((bf16[8,4,2688]{2,1,0:T(4,128)(2,1)}), bf16[8,4,2688]{2,1,0:T(4,128)(2,1)S(1)}, u32[]{:S(2)}, u32[]{:S(2)}) async-start(bf16[8,4,2688]{2,1,0:T(4,128)(2,1)} %fold.1), calls=%async_computation | async-start | bytes 344064 | tf_op jit(solution)/shard_map/all_to_all | solution.py:450
  25.6 2.0 %prepare.1 = (f32[1,16,64,128]{3,2,1,0:T(8,128)S(1)}, bf16[1024,128]{1,0:T(8,128)(2,1)S(1)}, bf16[1024,128]{1,0:T(8,128)(2,1)S(1)}, f32[3,1536]{1,0:T(4,128)S(1)...) custom-call(s32[1]{0:T(128)S(6)} %copy.24.accepted, ...), custom_call_target="tpu_custom_call" | custom-call | tf_op jit(solution)/shard_map/prepare/pallas_call | solution.py:186
  27.5 1.6 %all-to-all-done.arrived = bf16[8,4,2688]{2,1,0:T(4,128)(2,1)S(1)} async-done(((bf16[8,4,2688]{2,1,0:T(4,128)(2,1)}), bf16[8,4,2688]{2,1,0:T(4,128)(2,1)S(1)}, u32[]{:S(2)}, u32[]{:S(2)}) %all-to-all-start) | async-done | bytes 172064 | tf_op jit(solution)/shard_map/all_to_all | solution.py:450
  29.2 0.4 chain.1
  29.6 15.1 %all_to_all.10 = bf16[32,4,1024]{2,1,0:T(4,128)(2,1)S(1)} all-to-all(bf16[32,4,1024]{2,1,0:T(4,128)(2,1)S(1)} %get-tuple-element.38), channel_id=1, replica_groups={{36,38,32,34,44,46,40,42,52,54,48,50,60,62,56,58,4,6,0,2,12,14,8,10,20,..., dimensions={0} | all-to-all | bytes 524288 | tf_op jit(solution)/shard_map/all_to_all | solution.py:452
  44.7 0.1 reshape.29.rows
  44.8 0.0 copy-done
  44.8 0.3 output.1.mine
  45.0 2.8 %collective-permute-start.3 = (bf16[128,128]{1,0:T(8,128)(2,1)S(1)}, bf16[128,128]{1,0:T(8,128)(2,1)S(1)}, u32[]{:S(2)}, u32[]{:S(2)}) collective-permute-start(bf16[128,128]{1,0:T(8,128)(2,1)S(1)} %output.1.mine), channel_id=1, source_target_pairs={{0,1},{1,0},{2,3},{3,2},{4,5},{5,4},{6,7},{7,6},{8,9},{9,8},{10,11... | collective-permute-start | bytes 98312 | tf_op jit(solution)/shard_map/ppermute | solution.py:456
  47.9 2.5 %states.3 = (f32[1,5,16,64,128]{4,3,2,1,0:T(8,128)}, bf16[1,7,1024]{2,1,0:T(8,128)(2,1)}, bf16[1,7,256]{2,1,0:T(8,128)(2,1)}, bf16[1,7,256]{2,1,0:T(8,128)(2,1)}) custom-call(f32[1,16,64,128]{3,2,1,0:T(8,128)S(1)} %get-tuple-element.39.first, f32[8,1024]{1,0:T(8,128)S(1)} %get-tuple-element.40.moved, f32[4,256]{1,0:T(4,128)S(1)} %get-tuple-element.41.keys, ...), custom_call_target="tpu_custom_call" | custom-call | tf_op jit(solution)/shard_map/states/pallas_call | solution.py:345
  50.4 0.0 collective-permute-done.3.other
  50.4 0.8 %combine.1 = bf16[32,4,64]{2,1,0:T(4,128)(2,1)} custom-call(bf16[128,128]{1,0:T(8,128)(2,1)S(1)} %output.1.mine, bf16[128,128]{1,0:T(8,128)(2,1)S(1)} %collective-permute-done.3.other), custom_call_target="tpu_custom_call" | custom-call | tf_op jit(solution)/shard_map/combine/pallas_call | solution.py:401
Async XLA Ops:
  2.1 6.4 %collective-permute-start = (bf16[648,128]{1,0:T(8,128)(2,1)S(1)}, bf16[648,128]{1,0:T(8,128)(2,1)S(1)}, u32[]{:S(2)}, u32[]{:S(2)}) collective-permute-start(bf16[648,128]{1,0:T(8,128)(2,1)S(1)} %get-tuple-element.28), channel_id=1, source_target_pairs={{0,2},{2,4},{4,6},{6,0},{1,3},{3,5},{5,7},{7,1},{8,10},{10,12},{12... | collective-permute-start | bytes 497672 | tf_op jit(solution)/shard_map/ppermute | solution.py:439
  4.3 9.8 %collective-permute-start.1 = (bf16[648,128]{1,0:T(8,128)(2,1)S(1)}, bf16[648,128]{1,0:T(8,128)(2,1)S(1)}, u32[]{:S(2)}, u32[]{:S(2)}) collective-permute-start(bf16[648,128]{1,0:T(8,128)(2,1)S(1)} %get-tuple-element.29), channel_id=1, source_target_pairs={{0,4},{2,6},{4,0},{6,2},{1,5},{3,7},{5,1},{7,3},{8,12},{10,14},{12... | collective-permute-start | bytes 497672 | tf_op jit(solution)/shard_map/ppermute | solution.py:439
  6.9 7.2 %collective-permute-start.2 = (bf16[648,128]{1,0:T(8,128)(2,1)S(1)}, bf16[648,128]{1,0:T(8,128)(2,1)S(1)}, u32[]{:S(2)}, u32[]{:S(2)}) collective-permute-start(bf16[648,128]{1,0:T(8,128)(2,1)S(1)} %get-tuple-element.30), channel_id=1, source_target_pairs={{0,6},{2,0},{4,2},{6,4},{1,7},{3,1},{5,3},{7,5},{8,14},{10,8},{12,... | collective-permute-start | bytes 497672 | tf_op jit(solution)/shard_map/ppermute | solution.py:439
  15.0 29.8 %copy-start = (bf16[1024,64]{0,1:T(8,128)(2,1)S(1)}, bf16[1024,64]{0,1:T(8,128)(2,1)}, u32[]{:S(2)}) copy-start(bf16[1024,64]{0,1:T(8,128)(2,1)} %param.32) | copy-start | bytes 393220
  15.0 14.2 %all-to-all-start = ((bf16[8,4,2688]{2,1,0:T(4,128)(2,1)}), bf16[8,4,2688]{2,1,0:T(4,128)(2,1)S(1)}, u32[]{:S(2)}, u32[]{:S(2)}) async-start(bf16[8,4,2688]{2,1,0:T(4,128)(2,1)} %fold.1), calls=%async_computation | async-start | bytes 344064 | tf_op jit(solution)/shard_map/all_to_all | solution.py:450
  45.0 5.3 %collective-permute-start.3 = (bf16[128,128]{1,0:T(8,128)(2,1)S(1)}, bf16[128,128]{1,0:T(8,128)(2,1)S(1)}, u32[]{:S(2)}, u32[]{:S(2)}) collective-permute-start(bf16[128,128]{1,0:T(8,128)(2,1)S(1)} %output.1.mine), channel_id=1, source_target_pairs={{0,1},{1,0},{2,3},{3,2},{4,5},{5,4},{6,7},{7,6},{8,9},{9,8},{10,11... | collective-permute-start | bytes 98312 | tf_op jit(solution)/shard_map/ppermute | solution.py:456

commit v7 on v5

--- a/solution.py
+++ b/solution.py
@@ -353,9 +353,9 @@
     )(*map(local, (first, moved, keys, decay, rows, new)))
 
 
-def output_kernel(rows, w_out, gain, out):
+def output_kernel(blocks, w_out, gain, out):
     features = w_out.shape[0]
-    x = rows[...]
+    x = blocks[...].reshape(-1, blocks.shape[2])
     out[:, :features] = lax.dot_general(x, w_out[...], NT, preferred_element_type=F32).astype(BF16)
     wide = x.astype(F32)
     inverse = 1.0 / (gain[...] * gain[...])
@@ -371,7 +371,7 @@
         output_kernel,
         in_specs=[vmem] * 3,
         out_specs=vmem,
-        out_shape=VMEM((rows.shape[0], LANES), BF16),
+        out_shape=VMEM((rows.shape[0] * rows.shape[1], LANES), BF16),
         name="output",
     )(local(rows), local(w_out.T), local(gain))
 
@@ -419,10 +419,10 @@
     past_states,
     accepted,
 ):
-    group_seqs, proposals, features = tokens.shape
+    group_seqs, _, features = tokens.shape
     near, far = lax.axis_size("ky"), lax.axis_size("kz")
     far_order = [(far // 2 + 1 + i) % far for i in range(far)]
-    order = [(far // 2 + i) % far * near + (near // 2 + j) % near for i in range(far) for j in range(near)]
+    order = [(far // 2 + i) % far * near + (near // 2 + j) % near for j in range(near) for i in range(far)]
     weights = (w_gate, w_value, w_key, w_query, w_step)
     own, *others = project(tokens, in_gain, weights, near)
     nearby = {0: own}
@@ -442,7 +442,7 @@
     sent, moved, keys, decay, new = chain(group_seqs, arrived, high, low, base, taps, bias, rate, gain)
     gathered = lax.all_to_all(sent, KV, 0, 0, axis_index_groups=[order], tiled=True)
     saved = next_states(past_states.shape[1], first, moved, keys, decay, rows, new)
-    mine = output(gathered.reshape(group_seqs * proposals, -1), w_out, gain)
+    mine = output(gathered, w_out, gain)
     swap = [(i, 1 - i) for i in range(2)]
     mixed = combine(mine, lax.ppermute(mine, "tp", swap), order, features)
     return (mixed, *saved)

time: 51.8 us -> 51.5 us (level)
  no operation moved by 1% of the time
where the time goes in v7:
time: 51.5 us; the launch traced here: 51.2 us
  starting transfers between devices  18.1 us (35%)
  blocking collectives  15.5 us (30%)
  Pallas kernels  8.15 us (16%)
  waiting for transfers between devices  8.06 us (16%)
  between operations  1.34 us (3%)
    all_to_all x1, blocking collectives, per_device(): lax.all_to_all(sent, KV, 0, 0, axis_index_groups=[order], tiled=True)  15.5 us
    all_to_all x1, starting transfers between devices, per_device(): lax.all_to_all(partial, 'kz', 0, 0, axis_index_groups=[far_order], tiled=...  9.76 us
    ppermute x3, waiting for transfers between devices, per_device(): lax.ppermute(others[k - 1], 'ky', [(i, (i + k) % near) for i in range(nea...  6.41 us
    ppermute x3, starting transfers between devices, per_device(): lax.ppermute(others[k - 1], 'ky', [(i, (i + k) % near) for i in range(nea...  5.88 us
    pallas_call x1, Pallas kernels, next_states(): pl.pallas_call(states_kernel, in_specs=[vmem] * 6, out_specs=[pl.BlockSpe...  2.47 us
    ppermute x1, starting transfers between devices, per_device(): mixed = combine(mine, lax.ppermute(mine, 'tp', swap), order, features)  2.45 us
    pallas_call x1, Pallas kernels, prepare(): pl.pallas_call(prepare_kernel, in_specs=[pl.BlockSpec(memory_space=pltpu....  1.96 us
    all_to_all x1, waiting for transfers between devices, per_device(): lax.all_to_all(partial, 'kz', 0, 0, axis_index_groups=[far_order], tiled=...  1.65 us
  transfers between devices with their start and end apart: 5, of which 3 were waited for; matrix products, arithmetic and copies ran while one was open for 0% of the time, Pallas kernels for 9%

profile of v7, /device:TPU:1, one launch (start us, length us, event | category | flops | bytes accessed | tf_op | source)
XLA Modules:
  0.0 51.2 jit_solution(10450011915743332100)
XLA Ops:
  0.6 1.4 %project.1 = (bf16[32,2688]{1,0:T(8,128)(2,1)S(1)}, bf16[32,2688]{1,0:T(8,128)(2,1)S(1)}, bf16[32,2688]{1,0:T(8,128)(2,1)S(1)}, bf16[32,2688]{1,0:T(8,128)(2,1)S(1)}) custom-call(bf16[32,4,64]{2,1,0:T(4,128)(2,1)} %tok.1, f32[1,64]{1,0:T(1,128)} %bitcast.9, bf16[64,1024]{1,0:T(8,128)(2,1)} %wg.1, bf16[64,1024]{1,0:T(8,128)(2,1)} %wv.1, bf16[64,256]{1,0:T(8,128)(2,1)} %wk.1, ...), custom_call_target="tpu_custom_call" | custom-call | tf_op jit(solution)/shard_map/project/pallas_call | solution.py:80
  2.0 0.0 copy-start
  2.0 2.2 %collective-permute-start = (bf16[32,2688]{1,0:T(8,128)(2,1)S(1)}, bf16[32,2688]{1,0:T(8,128)(2,1)S(1)}, u32[]{:S(2)}, u32[]{:S(2)}) collective-permute-start(bf16[32,2688]{1,0:T(8,128)(2,1)S(1)} %get-tuple-element.28), channel_id=1, source_target_pairs={{0,2},{2,4},{4,6},{6,0},{1,3},{3,5},{5,7},{7,1},{8,10},{10,12},{12... | collective-permute-start | bytes 516104 | tf_op jit(solution)/shard_map/ppermute | solution.py:430
  4.2 2.6 %collective-permute-start.1 = (bf16[32,2688]{1,0:T(8,128)(2,1)S(1)}, bf16[32,2688]{1,0:T(8,128)(2,1)S(1)}, u32[]{:S(2)}, u32[]{:S(2)}) collective-permute-start(bf16[32,2688]{1,0:T(8,128)(2,1)S(1)} %get-tuple-element.29), channel_id=1, source_target_pairs={{0,4},{2,6},{4,0},{6,2},{1,5},{3,7},{5,1},{7,3},{8,12},{10,14},{12... | collective-permute-start | bytes 516104 | tf_op jit(solution)/shard_map/ppermute | solution.py:430
  6.8 1.1 %collective-permute-start.2 = (bf16[32,2688]{1,0:T(8,128)(2,1)S(1)}, bf16[32,2688]{1,0:T(8,128)(2,1)S(1)}, u32[]{:S(2)}, u32[]{:S(2)}) collective-permute-start(bf16[32,2688]{1,0:T(8,128)(2,1)S(1)} %get-tuple-element.30), channel_id=1, source_target_pairs={{0,6},{2,0},{4,2},{6,4},{1,7},{3,1},{5,3},{7,5},{8,14},{10,8},{12,... | collective-permute-start | bytes 516104 | tf_op jit(solution)/shard_map/ppermute | solution.py:430
  7.9 0.5 %collective-permute-done.refs_1_ = bf16[32,2688]{1,0:T(8,128)(2,1)S(1)} collective-permute-done((bf16[32,2688]{1,0:T(8,128)(2,1)S(1)}, bf16[32,2688]{1,0:T(8,128)(2,1)S(1)}, u32[]{:S(2)}, u32[]{:S(2)}) %collective-permute-start) | collective-permute-done | bytes 172064 | tf_op jit(solution)/shard_map/ppermute | solution.py:430
  8.4 5.9 %collective-permute-done.1.refs_2_ = bf16[32,2688]{1,0:T(8,128)(2,1)S(1)} collective-permute-done((bf16[32,2688]{1,0:T(8,128)(2,1)S(1)}, bf16[32,2688]{1,0:T(8,128)(2,1)S(1)}, u32[]{:S(2)}, u32[]{:S(2)}) %collective-permute-start.1) | collective-permute-done | bytes 172064 | tf_op jit(solution)/shard_map/ppermute | solution.py:430
  14.3 0.0 collective-permute-done.2.refs_3_
  14.3 0.9 %fold.1 = bf16[8,4,2688]{2,1,0:T(4,128)(2,1)} custom-call(bf16[32,2688]{1,0:T(8,128)(2,1)S(1)} %get-tuple-element.27.refs_0_, bf16[32,2688]{1,0:T(8,128)(2,1)S(1)} %collective-permute-done.refs_1_, bf16[32,2688]{1,0:T(8,128)(2,1)S(1)} %collective-permute-done.1.refs_2_, bf16[32,2688]{1,0:T(8,128)(2,1)S(1)} %collective-permute-done.2.refs_3_), custom_call_target="tpu_custom_call" | custom-call | tf_op jit(solution)/shard_map/fold/pallas_call | solution.py:108
  15.2 9.8 %all-to-all-start = ((bf16[8,4,2688]{2,1,0:T(4,128)(2,1)}), bf16[8,4,2688]{2,1,0:T(4,128)(2,1)S(1)}, u32[]{:S(2)}, u32[]{:S(2)}) async-start(bf16[8,4,2688]{2,1,0:T(4,128)(2,1)} %fold.1), calls=%async_computation | async-start | bytes 344064 | tf_op jit(solution)/shard_map/all_to_all | solution.py:441
  25.6 2.0 %prepare.1 = (f32[1,16,64,128]{3,2,1,0:T(8,128)S(1)}, bf16[1024,128]{1,0:T(8,128)(2,1)S(1)}, bf16[1024,128]{1,0:T(8,128)(2,1)S(1)}, f32[3,1536]{1,0:T(4,128)S(1)...) custom-call(s32[1]{0:T(128)S(6)} %copy.24.accepted, ...), custom_call_target="tpu_custom_call" | custom-call | tf_op jit(solution)/shard_map/prepare/pallas_call | solution.py:178
  27.6 1.6 %all-to-all-done.arrived = bf16[8,4,2688]{2,1,0:T(4,128)(2,1)S(1)} async-done(((bf16[8,4,2688]{2,1,0:T(4,128)(2,1)}), bf16[8,4,2688]{2,1,0:T(4,128)(2,1)S(1)}, u32[]{:S(2)}, u32[]{:S(2)}) %all-to-all-start) | async-done | bytes 172064 | tf_op jit(solution)/shard_map/all_to_all | solution.py:441
  29.2 0.4 chain.1
  29.6 15.5 %all_to_all.10.blocks = bf16[32,4,1024]{2,1,0:T(4,128)(2,1)S(1)} all-to-all(bf16[32,4,1024]{2,1,0:T(4,128)(2,1)S(1)} %get-tuple-element.38), channel_id=1, replica_groups={{36,44,52,60,4,12,20,28,38,46,54,62,6,14,22,30,32,40,48,56,0,8,16,24,34..., dimensions={0} | all-to-all | bytes 524288 | tf_op jit(solution)/shard_map/all_to_all | solution.py:443
  45.1 0.0 copy-done
  45.1 0.3 output.1.mine
  45.4 2.4 %collective-permute-start.3 = (bf16[128,128]{1,0:T(8,128)(2,1)S(1)}, bf16[128,128]{1,0:T(8,128)(2,1)S(1)}, u32[]{:S(2)}, u32[]{:S(2)}) collective-permute-start(bf16[128,128]{1,0:T(8,128)(2,1)S(1)} %output.1.mine), channel_id=1, source_target_pairs={{0,1},{1,0},{2,3},{3,2},{4,5},{5,4},{6,7},{7,6},{8,9},{9,8},{10,11... | collective-permute-start | bytes 98312 | tf_op jit(solution)/shard_map/ppermute | solution.py:447
  47.9 2.5 %states.3 = (f32[1,5,16,64,128]{4,3,2,1,0:T(8,128)}, bf16[1,7,1024]{2,1,0:T(8,128)(2,1)}, bf16[1,7,256]{2,1,0:T(8,128)(2,1)}, bf16[1,7,256]{2,1,0:T(8,128)(2,1)}) custom-call(f32[1,16,64,128]{3,2,1,0:T(8,128)S(1)} %get-tuple-element.39.first, f32[8,1024]{1,0:T(8,128)S(1)} %get-tuple-element.40.moved, f32[4,256]{1,0:T(4,128)S(1)} %get-tuple-element.41.keys, ...), custom_call_target="tpu_custom_call" | custom-call | tf_op jit(solution)/shard_map/states/pallas_call | solution.py:337
  50.3 0.0 collective-permute-done.3.other
  50.4 0.8 %combine.1 = bf16[32,4,64]{2,1,0:T(4,128)(2,1)} custom-call(bf16[128,128]{1,0:T(8,128)(2,1)S(1)} %output.1.mine, bf16[128,128]{1,0:T(8,128)(2,1)S(1)} %collective-permute-done.3.other), custom_call_target="tpu_custom_call" | custom-call | tf_op jit(solution)/shard_map/combine/pallas_call | solution.py:393
Async XLA Ops:
  2.0 43.1 %copy-start = (bf16[1024,64]{0,1:T(8,128)(2,1)S(1)}, bf16[1024,64]{0,1:T(8,128)(2,1)}, u32[]{:S(2)}) copy-start(bf16[1024,64]{0,1:T(8,128)(2,1)} %param.32) | copy-start | bytes 393220
  2.0 6.4 %collective-permute-start = (bf16[32,2688]{1,0:T(8,128)(2,1)S(1)}, bf16[32,2688]{1,0:T(8,128)(2,1)S(1)}, u32[]{:S(2)}, u32[]{:S(2)}) collective-permute-start(bf16[32,2688]{1,0:T(8,128)(2,1)S(1)} %get-tuple-element.28), channel_id=1, source_target_pairs={{0,2},{2,4},{4,6},{6,0},{1,3},{3,5},{5,7},{7,1},{8,10},{10,12},{12... | collective-permute-start | bytes 516104 | tf_op jit(solution)/shard_map/ppermute | solution.py:430
  4.2 10.1 %collective-permute-start.1 = (bf16[32,2688]{1,0:T(8,128)(2,1)S(1)}, bf16[32,2688]{1,0:T(8,128)(2,1)S(1)}, u32[]{:S(2)}, u32[]{:S(2)}) collective-permute-start(bf16[32,2688]{1,0:T(8,128)(2,1)S(1)} %get-tuple-element.29), channel_id=1, source_target_pairs={{0,4},{2,6},{4,0},{6,2},{1,5},{3,7},{5,1},{7,3},{8,12},{10,14},{12... | collective-permute-start | bytes 516104 | tf_op jit(solution)/shard_map/ppermute | solution.py:430
  6.8 7.5 %collective-permute-start.2 = (bf16[32,2688]{1,0:T(8,128)(2,1)S(1)}, bf16[32,2688]{1,0:T(8,128)(2,1)S(1)}, u32[]{:S(2)}, u32[]{:S(2)}) collective-permute-start(bf16[32,2688]{1,0:T(8,128)(2,1)S(1)} %get-tuple-element.30), channel_id=1, source_target_pairs={{0,6},{2,0},{4,2},{6,4},{1,7},{3,1},{5,3},{7,5},{8,14},{10,8},{12,... | collective-permute-start | bytes 516104 | tf_op jit(solution)/shard_map/ppermute | solution.py:430
  15.2 14.0 %all-to-all-start = ((bf16[8,4,2688]{2,1,0:T(4,128)(2,1)}), bf16[8,4,2688]{2,1,0:T(4,128)(2,1)S(1)}, u32[]{:S(2)}, u32[]{:S(2)}) async-start(bf16[8,4,2688]{2,1,0:T(4,128)(2,1)} %fold.1), calls=%async_computation | async-start | bytes 344064 | tf_op jit(solution)/shard_map/all_to_all | solution.py:441
  45.4 4.9 %collective-permute-start.3 = (bf16[128,128]{1,0:T(8,128)(2,1)S(1)}, bf16[128,128]{1,0:T(8,128)(2,1)S(1)}, u32[]{:S(2)}, u32[]{:S(2)}) collective-permute-start(bf16[128,128]{1,0:T(8,128)(2,1)S(1)} %output.1.mine), channel_id=1, source_target_pairs={{0,1},{1,0},{2,3},{3,2},{4,5},{5,4},{6,7},{7,6},{8,9},{9,8},{10,11... | collective-permute-start | bytes 98312 | tf_op jit(solution)/shard_map/ppermute | solution.py:447
